TPU v7x, 256 devices: a whole 4x4x8 slice. The times are simulated.
256 devices in a mesh: sp: 32 (over z, x), tp: 8 (over y, core).
Axes of the slice: x: 4, y: 4, z: 8, core: 2. Of those that a mesh axis runs over, the one named last changes fastest.
Arguments:
- tokens: bfloat16 [8192, 4096], P('sp', 'tp'), may hold values from -6 to 6
- pre_gain: float32 [4096], replicated, may hold values from 0.1 to 1.9
- rate_factor: float32 [8192], P('sp'), may hold values from 0.5 to 2, as said below
- w_rec_in: bfloat16 [4096, 1024], P(None, 'tp'), may hold values from -0.09375 to 0.09375
- w_rec_gate: bfloat16 [4096, 1024], P(None, 'tp')
- conv_taps: float32 [4, 1024], P(None, 'tp'), may hold values from -3 to 3
- rate_maps: bfloat16 [8, 128, 128], P('tp'), may hold values from -0.5 to 0.5
- input_maps: bfloat16 [8, 128, 128], P('tp'), may hold values from -0.5 to 0.5
- decay_param: float32 [1024], P('tp'), as said below
- w_query: bfloat16 [4096, 1536], P(None, 'tp'), may hold values from -0.09375 to 0.09375
- w_latent: bfloat16 [4096, 512], replicated, may hold values from -0.09375 to 0.09375
- w_rope_key: bfloat16 [4096, 64], replicated, may hold values from -0.09375 to 0.09375
- latent_gain: float32 [512], replicated, may hold values from 0.7 to 100, as said below
- w_expand: bfloat16 [512, 2048], P(None, 'tp')
- rec_gain: float32 [1024], P('tp'), may hold values from 0.1 to 1.9
- att_gain: float32 [1024], P('tp'), may hold values from 0.1 to 1.9
- w_out_rec: bfloat16 [1024, 4096], P('tp'), may hold values from -0.125 to 0.125
- w_out_att: bfloat16 [1024, 4096], P('tp'), may hold values from -0.125 to 0.125
- post_gain: float32 [4096], replicated, may hold values from 0.1 to 1.9
Outputs:
- layer_out: bfloat16 [8192, 4096], P(('sp', 'tp'))
Inputs may be any that keep to these rules, and one draw needn't show every extreme that they name: `rate_factor`: one positive factor for each position. `decay_param`: one parameter for each recurrent channel. `latent_gain`: one positive gain for each latent entry.
All inputs are finite; a program needn't handle non-finite values.
Results may differ from a plain program's by a relative error of at most 0.017.
The roundings to bfloat16 on the way count: a program that leaves them out, or rounds other values in their place, can miss the bound.
Values may be sent and summed in bfloat16 or wider, within the bound.
A program may use at most 128 MiB of HBM per device.

v0:
```python
import math

import jax
import jax.numpy as jnp
from jax import lax
from jax.sharding import PartitionSpec as P

NOPE = 128
ROPE = 64
VDIM = 128


EPS = 1e-06
RATE_C = 8.0
THETA = 10000.0
span_limit = 2048


def passed_along(block, axis, distance):
    devices = range(lax.axis_size(axis))
    route = [(i - distance, i) for i in devices if i - distance in devices]
    return lax.ppermute(block, axis, route)


def from_everyone(shard, axis):
    copies = jnp.broadcast_to(shard, (lax.axis_size(axis), *shard.shape))
    return lax.all_to_all(copies, axis, split_axis=0, concat_axis=0, tiled=True)


def all_in_one(shard, axis):
    leaves = jax.tree.leaves(shard)
    order = sorted(range(len(leaves)), key=lambda k: -leaves[k].size)
    width = (1, *leaves[order[0]].shape)[-1]
    lines = [
        jnp.pad(leaves[k].reshape(-1), (0, -leaves[k].size % width)).reshape(-1, width)
        for k in order
    ]
    both, at, found = (from_everyone(jnp.concatenate(lines), axis), 0, {})
    for k, line in zip(order, lines):
        slab = both[:, at : at + len(line)].reshape(len(both), -1)
        found[k] = slab[:, : leaves[k].size].reshape(-1, *leaves[k].shape)
        at += len(line)
    numbers = iter(range(len(leaves)))
    return jax.tree.map(lambda _: found[next(numbers)], shard)


def joined_by_halves(pieces, combine):
    while len(jax.tree.leaves(pieces)[0]) > 1:
        pieces = jax.vmap(combine)(
            *(jax.tree.map(lambda part: part[side::2], pieces) for side in (0, 1))
        )
    return jax.tree.map(lambda part: part[0], pieces)


def entering(shard, axis, combine, identity):
    count, mine = (lax.axis_size(axis), lax.axis_index(axis))
    passed = jnp.arange(count) < mine

    def kept(part, zero, own):
        part = jnp.where(
            passed.reshape(-1, *(1 for _ in own.shape)), part, jnp.asarray(zero, own.dtype)
        )
        return part

    pieces = all_in_one(shard, axis)
    return joined_by_halves(jax.tree.map(kept, pieces, identity, shard), combine)


def of_everyone(shard, axis):
    return from_everyone(shard, axis).sum(axis=0)


def in_one_piece(arrays, axis, dim, along):
    widths = [a.shape[along] for a in arrays]
    both = jnp.concatenate(arrays, axis=along)
    out = lax.all_gather(both, axis, axis=dim, tiled=True)
    return tuple(jnp.split(out, [sum(widths[:k]) for k in range(1, len(widths))], axis=along))


def in_blocks(shard, dim, count):
    before, after = (shard.shape[:dim], shard.shape[dim + 1 :])
    return jnp.moveaxis(shard.reshape(*before, count, -1, *after), dim, 0)


def sum_at_owner(shard, axis, dim):
    count = lax.axis_size(axis)
    pieces = lax.all_to_all(in_blocks(shard, dim, count), axis, 0, 0, tiled=True)
    return jnp.sum(pieces.astype(jnp.float32), axis=0)


def rms_inverse(values):
    return lax.rsqrt(jnp.mean(values * values, axis=-1, keepdims=True) + EPS)


def rotate(values, cosine, sine_part):
    half_width = values.shape[-1] // 2
    leading = values[..., :half_width]
    trailing = values[..., half_width:]
    return jnp.concatenate(
        [leading * cosine - trailing * sine_part, trailing * cosine + leading * sine_part], axis=-1
    )


def angles(length, offset, span_width):
    frequency = 1.0 / THETA ** (jnp.arange(0, span_width, 2).astype(jnp.float32) / span_width)
    places = (offset + jnp.arange(length)).astype(jnp.float32)
    turned = places[:, None] * frequency[None, :]
    return (jnp.cos(turned), jnp.sin(turned))


def combine_steps(earlier, later):
    return (earlier[0] * later[0], later[0] * earlier[1] + later[1])


def attend_block(state_now, query_nope, query_rope, places, keys_nope, key_rope, values, key_root):
    maxima, totals, accumulated = state_now
    scaling = 1.0 / math.sqrt(query_nope.shape[-1] + query_rope.shape[-1])
    scores = jnp.einsum("qhd,khd->hqk", query_nope, keys_nope, preferred_element_type=jnp.float32)
    scores = scores + jnp.einsum(
        "qhd,kd->hqk", query_rope, key_rope, preferred_element_type=jnp.float32
    )
    scores = scores * scaling
    key_places = key_root + jnp.arange(keys_nope.shape[0])
    visible = key_places[None, :] <= places[:, None]
    scores = jnp.where(visible[None], scores, -jnp.inf)
    largest = jnp.maximum(maxima, jnp.max(scores, axis=-1))
    anchor = jnp.where(largest == -jnp.inf, 0.0, largest)
    weights = jnp.exp(scores - anchor[..., None])
    shrink = jnp.exp(maxima - anchor)
    totals = totals * shrink + jnp.sum(weights, axis=-1)
    accumulated = accumulated * shrink[..., None] + jnp.einsum(
        "hqk,khd->hqd", weights.astype(jnp.bfloat16), values, preferred_element_type=jnp.float32
    )
    return (largest, totals, accumulated)


def shards(
    tokens,
    pre_gain,
    rate_factor,
    w_rec_in,
    w_rec_gate,
    conv_taps,
    rate_maps,
    input_maps,
    decay_param,
    w_query,
    w_latent,
    w_rope_key,
    latent_gain,
    w_expand,
    rec_gain,
    att_gain,
    w_out_rec,
    w_out_att,
    post_gain,
):
    row_count = tokens.shape[0]
    model_width = w_rec_in.shape[0]
    channels = w_rec_in.shape[1]
    heads_here = w_query.shape[1] // (NOPE + ROPE)
    group_size = lax.axis_size("tp")
    first_place = lax.axis_index("sp") * row_count
    places = first_place + jnp.arange(row_count)
    last_place = first_place + row_count - 1
    piece_wide = lax.all_gather(tokens, "tp", axis=1, tiled=True).astype(jnp.float32)
    piece_low = (piece_wide * pre_gain).astype(jnp.bfloat16)

    def accumulate(source, weight):
        return jnp.dot(source, weight, preferred_element_type=jnp.float32)

    squares = jnp.sum(piece_wide * piece_wide, axis=1, keepdims=True)
    sum_input = accumulate(piece_low, w_rec_in)
    sum_gate = accumulate(piece_low, w_rec_gate)
    sum_query = accumulate(piece_low, w_query)
    sum_latent = accumulate(piece_low, w_latent)
    sum_rope = accumulate(piece_low, w_rope_key)
    inverse = lax.rsqrt(squares / model_width + EPS)
    rec_input = (inverse * sum_input).astype(jnp.bfloat16)
    gate_value = inverse * sum_gate
    query_raw = inverse * sum_query
    latent_raw = inverse * sum_latent
    rope_raw = inverse * sum_rope
    taps = conv_taps.shape[0]
    tail_rows = rec_input[row_count - (taps - 1) :]
    before = passed_along(tail_rows, "sp", 1)
    padded = jnp.concatenate([before, rec_input], axis=0)
    convolved = conv_taps[0] * padded[0:row_count].astype(jnp.float32)
    for tap_index in range(1, taps):
        convolved = convolved + conv_taps[tap_index] * padded[
            tap_index : tap_index + row_count
        ].astype(jnp.float32)
    conv_low = convolved.astype(jnp.bfloat16)
    blocks = conv_low.reshape(row_count, rate_maps.shape[0], rate_maps.shape[1])
    rate_gate = jax.nn.sigmoid(
        jnp.einsum("sbi,bij->sbj", blocks, rate_maps, preferred_element_type=jnp.float32)
    ).reshape(row_count, channels)
    entry_gate = jax.nn.sigmoid(
        jnp.einsum("sbi,bij->sbj", blocks, input_maps, preferred_element_type=jnp.float32)
    ).reshape(row_count, channels)
    log_keep = -RATE_C * rate_factor[:, None] * rate_gate * jax.nn.softplus(-decay_param)
    keep_rate = jnp.exp(log_keep)
    driven = jnp.sqrt(-jnp.expm1(2.0 * log_keep)) * entry_gate * convolved
    cum_keep, local_state = lax.associative_scan(combine_steps, (keep_rate, driven), axis=0)
    identity = (jnp.ones((channels,), jnp.float32), jnp.zeros((channels,), jnp.float32))
    chain_keep, carried = entering(
        (cum_keep[row_count - 1], local_state[row_count - 1]), "sp", combine_steps, identity
    )
    state_seq = local_state + cum_keep * carried[None, :]
    rec_out = state_seq * jax.nn.gelu(gate_value)
    rec_squares = jnp.sum(rec_out * rec_out, axis=1, keepdims=True)
    rec_total = of_everyone(rec_squares, "tp")
    cosine, sine_part = angles(row_count, first_place, ROPE)
    query_heads = query_raw.reshape(row_count, heads_here, NOPE + ROPE)
    query_nope = query_heads[:, :, :NOPE].astype(jnp.bfloat16)
    query_rope = rotate(query_heads[:, :, NOPE:], cosine[:, None, :], sine_part[:, None, :]).astype(
        jnp.bfloat16
    )
    own_latent = (latent_raw * rms_inverse(latent_raw) * latent_gain).astype(jnp.bfloat16)
    rope_key = rotate(rope_raw, cosine, sine_part).astype(jnp.bfloat16)
    start_state = (
        jnp.full((heads_here, row_count), -jnp.inf, jnp.float32),
        jnp.zeros((heads_here, row_count), jnp.float32),
        jnp.zeros((heads_here, row_count, VDIM), jnp.float32),
    )
    expanded_local = jnp.dot(own_latent, w_expand, preferred_element_type=jnp.float32).astype(
        jnp.bfloat16
    )
    key_source, rope_source = in_one_piece((expanded_local, rope_key), "sp", 0, 1)
    total_rows = key_source.shape[0]
    key_span = math.gcd(total_rows, span_limit)

    def one_span(span_index, state_inner):
        key_root = span_index * key_span

        def compute(state_deep):
            source_rows = lax.dynamic_slice_in_dim(key_source, span_index * key_span, key_span, 0)
            rope_rows = lax.dynamic_slice_in_dim(rope_source, span_index * key_span, key_span, 0)
            expanded = source_rows
            expanded = expanded.reshape(key_span, heads_here, NOPE + VDIM)
            return attend_block(
                state_deep,
                query_nope,
                query_rope,
                places,
                expanded[:, :, :NOPE],
                rope_rows,
                expanded[:, :, NOPE:],
                key_root,
            )

        def keep_state(state_deep):
            return state_deep

        return lax.cond(key_root <= last_place, compute, keep_state, state_inner)

    maxima, totals, accumulated = lax.fori_loop(0, total_rows // key_span, one_span, start_state)
    att_out = (
        (accumulated / totals[..., None]).transpose(1, 0, 2).reshape(row_count, heads_here * VDIM)
    )
    att_squares = jnp.sum(att_out * att_out, axis=1, keepdims=True)
    att_total = of_everyone(att_squares, "tp")
    rec_norm = (rec_out * lax.rsqrt(rec_total / (channels * group_size) + EPS) * rec_gain).astype(
        jnp.bfloat16
    )
    att_norm = (
        att_out * lax.rsqrt(att_total / (heads_here * VDIM * group_size) + EPS) * att_gain
    ).astype(jnp.bfloat16)
    mixed_sum = sum_at_owner(
        (
            jnp.dot(rec_norm, w_out_rec, preferred_element_type=jnp.float32)
            + jnp.dot(att_norm, w_out_att, preferred_element_type=jnp.float32)
        ).astype(jnp.bfloat16),
        "tp",
        0,
    )
    return (mixed_sum * rms_inverse(mixed_sum) * post_gain).astype(jnp.bfloat16)


def solution(mesh):
    placed = (
        P("sp", "tp"),
        P(),
        P("sp"),
        P(None, "tp"),
        P(None, "tp"),
        P(None, "tp"),
        P("tp", None, None),
        P("tp", None, None),
        P("tp"),
        P(None, "tp"),
        P(),
        P(),
        P(),
        P(None, "tp"),
        P("tp"),
        P("tp"),
        P("tp", None),
        P("tp", None),
        P(),
    )
    return jax.shard_map(
        shards, mesh=mesh, in_specs=placed, out_specs=P(("sp", "tp"), None), check_vma=False
    )
```

profile of v0, /device:TPU:228, one launch (start us, length us, event | category | flops | bytes accessed | tf_op | source)
XLA Modules:
  0.0 218.6 jit_solution(17442014184566971345)
XLA Ops:
  7.3 30.1 %all-gather.3.cloned.1.call-done = bf16[256,4096]{1,0:T(8,128)(2,1)} async-done(((bf16[256,512]{1,0:T(8,128)(2,1)}), bf16[256,4096]{1,0:T(8,128)(2,1)}) %all-gather.3.cloned.1.call-update) | async-done | bytes 2097168 | tf_op jit(solution)/shard_map/all_gather | solution.py:166
  37.5 2.2 %fusion.16 = f32[256]{0:T(256)S(1)} fusion(bf16[256,4096]{1,0:T(8,128)(2,1)} %all-gather.3.cloned.1.call-done), kind=kLoop, calls=%fused_computation.29 | loop fusion | flops 3145472 | bytes 2098176 | tf_op jit(solution)/shard_map/reduce_sum | solution.py:172
  39.7 3.6 %multiply_reduce_fusion.1 = (f32[256]{0:T(256)S(1)}, f32[256,512]{1,0:T(8,128)S(1)}) fusion(bf16[4096,512]{1,0:T(8,128)(2,1)} %param.33, bf16[256,4096]{1,0:T(8,128)(2,1)S(1)} %copy-done.1, f32[4096]{0:T(1024)S(1)} %copy-done.14, f32[256]{0:T(256)S(1)} %add_rsqrt_fusion.3), kind=kOutput, calls=%fused_computation.55 | convolution fusion | flops 1077280512 | bytes 6834176 | tf_op jit(solution)/shard_map/dot_general | solution.py:170
  45.6 2.7 %fusion.29 = bf16[256,128]{1,0:T(8,128)(2,1)S(1)} fusion(bf16[4096,128]{1,0:T(8,128)(2,1)} %param.26, bf16[256,4096]{1,0:T(8,128)(2,1)} %all-gather.3.cloned.1.call-done, f32[4096]{0:T(1024)S(1)} %copy-done.14, f32[256]{0:T(256)S(1)} %add_rsqrt_fusion.3), kind=kOutput, calls=%fused_computation.50 | convolution fusion | flops 271646720 | bytes 3228672 | tf_op jit(solution)/shard_map/dot_general | solution.py:170
  48.3 3.1 %collective-permute-start = (bf16[3,128]{1,0:T(4,128)(2,1)S(1)}, bf16[3,128]{1,0:T(4,128)(2,1)S(1)}, u32[]{:S(2)}, u32[]{:S(2)}) collective-permute-start(bf16[3,128]{1,0:T(4,128)(2,1)S(1)} %slice.463), channel_id=1, source_target_pairs={{0,8},{8,16},{16,24},{24,32},{32,40},{40,48},{48,56},{56,64},{64,7... | collective-permute-start | bytes 2312 | tf_op jit(solution)/shard_map/ppermute | solution.py:22
  56.8 10.5 %all-to-all-start = ((f32[32,2,128]{2,1,0:T(2,128)}), f32[32,2,128]{2,1,0:T(2,128)S(1)}, u32[]{:S(2)}, u32[]{:S(2)}) async-start(f32[32,2,128]{2,1,0:T(2,128)} %broadcast_in_dim.42), calls=%async_computation | async-start | bytes 65536 | tf_op jit(solution)/shard_map/all_to_all | solution.py:27
  67.5 5.4 %all-to-all-done = f32[32,2,128]{2,1,0:T(2,128)S(1)} async-done(((f32[32,2,128]{2,1,0:T(2,128)}), f32[32,2,128]{2,1,0:T(2,128)S(1)}, u32[]{:S(2)}, u32[]{:S(2)}) %all-to-all-start) | async-done | bytes 32800 | tf_op jit(solution)/shard_map/all_to_all | solution.py:27
  73.3 2.7 %multiply_reduce_fusion.2 = (f32[256]{0:T(256)S(1)}, f32[256,128]{1,0:T(8,128)S(1)}) fusion(bf16[4096,128]{1,0:T(8,128)(2,1)} %param.27, bf16[256,4096]{1,0:T(8,128)(2,1)} %all-gather.3.cloned.1.call-done, f32[4096]{0:T(1024)S(1)} %copy-done.14, f32[256]{0:T(256)S(1)} %add_rsqrt_fusion.3, f32[128]{0:T(128)S(1)} %add_bitcast_fusion, ...), kind=kOutput, calls=%fused_computation.75 | convolution fusion | flops 272105216 | bytes 3820032 | tf_op jit(solution)/shard_map/dot_general | solution.py:170
  76.6 3.4 %all-to-all-start.1 = ((f32[8,256,1]{1,2,0:T(1,128)}), f32[8,256,1]{1,2,0:T(1,128)S(1)}, u32[]{:S(2)}, u32[]{:S(2)}) async-start(f32[8,256,1]{1,2,0:T(1,128)} %broadcast_in_dim.45), calls=%async_computation.1 | async-start | bytes 16384 | tf_op jit(solution)/shard_map/all_to_all | solution.py:27
  80.2 5.2 %all-to-all-done.1 = f32[8,256,1]{1,2,0:T(1,128)S(1)} async-done(((f32[8,256,1]{1,2,0:T(1,128)}), f32[8,256,1]{1,2,0:T(1,128)S(1)}, u32[]{:S(2)}, u32[]{:S(2)}) %all-to-all-start.1) | async-done | bytes 8224 | tf_op jit(solution)/shard_map/all_to_all | solution.py:27
  85.4 49.2 %all-gather.5.cloned.1.call-done = bf16[8192,320]{0,1:T(8,128)(2,1)} async-done(((bf16[256,320]{0,1:T(8,128)(2,1)}), bf16[8192,320]{0,1:T(8,128)(2,1)}) %all-gather.5.cloned.1.call-update) | async-done | bytes 5242896 | tf_op jit(solution)/shard_map/all_gather | solution.py:76
  134.6 4.7 %split.8 = bf16[8192,256]{0,1:T(8,128)(2,1)} slice(bf16[8192,320]{0,1:T(8,128)(2,1)} %all-gather.5.cloned.1.call-done), slice={[0:8192], [0:256]} | slice | bytes 8388608 | tf_op jit(solution)/shard_map/split | solution.py:77
  139.3 6.4 %copy.31 = bf16[8192,256]{1,0:T(8,128)(2,1)} copy(bf16[8192,256]{0,1:T(8,128)(2,1)} %split.8) | data formatting | bytes 8388608
  146.9 1.8 copy.33
  148.7 17.6 %while.18 = (s32[]{:T(128)}, f32[1,256]{1,0:T(1,128)S(1)}, f32[1,256]{1,0:T(1,128)S(1)}, f32[1,256,128]{2,1,0:T(8,128)S(1)}, s32[]{:T(128)}, /*index=5*/bf16[819...) while((s32[]{:T(128)}, f32[1,256]{1,0:T(1,128)S(1)}, ...), condition=%wide.region_9.10_spmd.clone, body=%wide.region_4.9_spmd.clone.sunk | while | flops 340332288 | bytes 14554469 | solution.py:257
  148.7 4.4 %conditional.3 = ((f32[1,256]{1,0:T(1,128)S(1)}, f32[1,256]{1,0:T(1,128)S(1)}, f32[1,256,128]{2,1,0:T(8,128)S(1)})) conditional(s32[]{:T(128)} %convert_element_type.205, (f32[1,256]{1,0:T(1,128)S(1)}, f32[1,256]{1,0:T(1,128)S(1)}, f32[1,256,128]{2,1,0:T(8,128)S(1)}) %tuple.82, (s32[]{:T(128)}, s32[]{:T(128)}, s32[]{:T(128)}, ...), branch_computations={%region_5.5_spmd, %region_6.8_spmd} | conditional | flops 340332288 | bytes 14553182 | solution.py:255
  153.1 4.3 %conditional.3 = ((f32[1,256]{1,0:T(1,128)S(1)}, f32[1,256]{1,0:T(1,128)S(1)}, f32[1,256,128]{2,1,0:T(8,128)S(1)})) conditional(s32[]{:T(128)} %convert_element_type.205, (f32[1,256]{1,0:T(1,128)S(1)}, f32[1,256]{1,0:T(1,128)S(1)}, f32[1,256,128]{2,1,0:T(8,128)S(1)}) %tuple.82, (s32[]{:T(128)}, s32[]{:T(128)}, s32[]{:T(128)}, ...), branch_computations={%region_5.5_spmd, %region_6.8_spmd} | conditional | flops 340332288 | bytes 14553182 | solution.py:255
  157.5 4.4 %conditional.3 = ((f32[1,256]{1,0:T(1,128)S(1)}, f32[1,256]{1,0:T(1,128)S(1)}, f32[1,256,128]{2,1,0:T(8,128)S(1)})) conditional(s32[]{:T(128)} %convert_element_type.205, (f32[1,256]{1,0:T(1,128)S(1)}, f32[1,256]{1,0:T(1,128)S(1)}, f32[1,256,128]{2,1,0:T(8,128)S(1)}) %tuple.82, (s32[]{:T(128)}, s32[]{:T(128)}, s32[]{:T(128)}, ...), branch_computations={%region_5.5_spmd, %region_6.8_spmd} | conditional | flops 340332288 | bytes 14553182 | solution.py:255
  158.9 1.5 convolution_bitcast_fusion
  161.9 4.3 %conditional.3 = ((f32[1,256]{1,0:T(1,128)S(1)}, f32[1,256]{1,0:T(1,128)S(1)}, f32[1,256,128]{2,1,0:T(8,128)S(1)})) conditional(s32[]{:T(128)} %convert_element_type.205, (f32[1,256]{1,0:T(1,128)S(1)}, f32[1,256]{1,0:T(1,128)S(1)}, f32[1,256,128]{2,1,0:T(8,128)S(1)}) %tuple.82, (s32[]{:T(128)}, s32[]{:T(128)}, s32[]{:T(128)}, ...), branch_computations={%region_5.5_spmd, %region_6.8_spmd} | conditional | flops 340332288 | bytes 14553182 | solution.py:255
  167.1 4.3 %all-to-all-start.2 = ((f32[8,256,1]{1,2,0:T(1,128)}), f32[8,256,1]{1,2,0:T(1,128)S(1)}, u32[]{:S(2)}, u32[]{:S(2)}) async-start(f32[8,256,1]{1,2,0:T(1,128)} %broadcast_in_dim.72), calls=%async_computation.2 | async-start | bytes 16384 | tf_op jit(solution)/shard_map/all_to_all | solution.py:27
  171.4 4.0 %fusion.54 = f32[256,4096]{1,0:T(8,128)} fusion(bf16[128,4096]{1,0:T(8,128)(2,1)} %param.39, f32[256,128]{1,0:T(8,128)S(1)} %get-tuple-element.364, f32[128]{0:T(128)S(1)} %copy-done.7, f32[256]{0:T(256)S(1)} %add_rsqrt_fusion.2), kind=kOutput, calls=%fused_computation.81 | convolution fusion | flops 268533760 | bytes 5375488 | tf_op jit(solution)/shard_map/dot_general | solution.py:271
  176.7 3.0 %fusion.15 = bf16[256,4096]{1,0:T(8,128)(2,1)S(1)} fusion(f32[256,4096]{1,0:T(8,128)} %fusion.54, bf16[128,4096]{1,0:T(8,128)(2,1)S(1)} %copy-done.3, f32[128]{0:T(128)S(1)} %copy-done.10, f32[256]{0:T(256)S(1)} %add_rsqrt_fusion, f32[1,256,128]{2,1,0:T(8,128)S(1)} %get-tuple-element.220, f32[256]{0:T(256)S(1)} %bitcast.96), kind=kOutput, calls=%fused_computation.28 | convolution fusion | flops 270663680 | bytes 7473664 | tf_op jit(solution)/shard_map/dot_general | solution.py:272
  179.7 30.5 %all_to_all.20 = bf16[8,32,4096]{2,1,0:T(8,128)(2,1)S(1)} all-to-all(bf16[8,32,4096]{2,1,0:T(8,128)(2,1)S(1)} %bitcast.87), channel_id=1, replica_groups=mesh['sp'=32,'tp'=8] {'tp'}, dimensions={0} | all-to-all | bytes 4194304 | tf_op jit(solution)/shard_map/all_to_all | solution.py:87
  (266 shorter events, 29.5 us)
Async XLA Ops:
  6.5 44.8 %copy-start = (bf16[4096,192]{0,1:T(8,128)(2,1)S(1)}, bf16[4096,192]{0,1:T(8,128)(2,1)}, u32[]{:S(2)}) copy-start(bf16[4096,192]{0,1:T(8,128)(2,1)} %param.32) | copy-start | bytes 4718596
  6.5 33.2 %copy-start.14 = (f32[4096]{0:T(1024)S(1)}, f32[4096]{0:T(1024)}, u32[]{:S(2)}) copy-start(f32[4096]{0:T(1024)} %param.24) | copy-start | bytes 49156
  6.5 30.9 %all-gather.3.cloned.1.call-start = ((), (), s32[]{:S(2)}) async-start(), calls=%async_computation.4 | async-start | bytes 2359296 | tf_op jit(solution)/shard_map/all_gather | solution.py:166
  7.3 127.3 %all-gather.5.cloned.1.call-start = ((), (), s32[]{:S(2)}) async-start(), calls=%async_computation.5 | async-start | bytes 5406720 | tf_op jit(solution)/shard_map/all_gather | solution.py:76
  37.5 2.3 %copy-start.1 = (bf16[256,4096]{1,0:T(8,128)(2,1)S(1)}, bf16[256,4096]{1,0:T(8,128)(2,1)}, u32[]{:S(2)}) copy-start(bf16[256,4096]{1,0:T(8,128)(2,1)} %all-gather.3.cloned.1.call-done) | copy-start | bytes 6291460
  39.7 3.6 %copy-start.11 = (bf16[4096,64]{0,1:T(8,128)(2,1)S(1)}, bf16[4096,64]{0,1:T(8,128)(2,1)}, u32[]{:S(2)}) copy-start(bf16[4096,64]{0,1:T(8,128)(2,1)} %param.34) | copy-start | bytes 1572868
  43.3 1.1 copy-start.4
  43.3 1.1 copy-start.6
  43.4 2.1 copy-start.15
  43.4 2.1 copy-start.9
  43.4 2.1 copy-start.8
  45.5 5.9 %copy-start.2 = (bf16[256,4096]{1,0:T(8,128)(2,1)S(1)}, bf16[256,4096]{1,0:T(8,128)(2,1)}, u32[]{:S(2)}) copy-start(bf16[256,4096]{1,0:T(8,128)(2,1)} %all-gather.3.cloned.1.call-done) | copy-start | bytes 6291460
  48.3 5.5 %copy-start.12 = (bf16[1,128,128]{2,1,0:T(8,128)(2,1)S(1)}, bf16[1,128,128]{2,1,0:T(8,128)(2,1)}, u32[]{:S(2)}) copy-start(bf16[1,128,128]{2,1,0:T(8,128)(2,1)} %param.29) | copy-start | bytes 98308
  48.3 5.7 %copy-start.13 = (bf16[1,128,128]{2,1,0:T(8,128)(2,1)S(1)}, bf16[1,128,128]{2,1,0:T(8,128)(2,1)}, u32[]{:S(2)}) copy-start(bf16[1,128,128]{2,1,0:T(8,128)(2,1)} %param.30) | copy-start | bytes 98308
  48.3 5.5 %collective-permute-start = (bf16[3,128]{1,0:T(4,128)(2,1)S(1)}, bf16[3,128]{1,0:T(4,128)(2,1)S(1)}, u32[]{:S(2)}, u32[]{:S(2)}) collective-permute-start(bf16[3,128]{1,0:T(4,128)(2,1)S(1)} %slice.463), channel_id=1, source_target_pairs={{0,8},{8,16},{16,24},{24,32},{32,40},{40,48},{48,56},{56,64},{64,7... | collective-permute-start | bytes 2312 | tf_op jit(solution)/shard_map/ppermute | solution.py:22
  56.8 16.1 %all-to-all-start = ((f32[32,2,128]{2,1,0:T(2,128)}), f32[32,2,128]{2,1,0:T(2,128)S(1)}, u32[]{:S(2)}, u32[]{:S(2)}) async-start(f32[32,2,128]{2,1,0:T(2,128)} %broadcast_in_dim.42), calls=%async_computation | async-start | bytes 65536 | tf_op jit(solution)/shard_map/all_to_all | solution.py:27
  76.6 8.7 %all-to-all-start.1 = ((f32[8,256,1]{1,2,0:T(1,128)}), f32[8,256,1]{1,2,0:T(1,128)S(1)}, u32[]{:S(2)}, u32[]{:S(2)}) async-start(f32[8,256,1]{1,2,0:T(1,128)} %broadcast_in_dim.45), calls=%async_computation.1 | async-start | bytes 16384 | tf_op jit(solution)/shard_map/all_to_all | solution.py:27
  145.7 1.2 slice-start
  148.7 22.7 %copy-start.7 = (f32[128]{0:T(128)S(1)}, f32[128]{0:T(128)}, u32[]{:S(2)}) copy-start(f32[128]{0:T(128)} %param.37) | copy-start | bytes 1540
  167.1 9.6 %all-to-all-start.2 = ((f32[8,256,1]{1,2,0:T(1,128)}), f32[8,256,1]{1,2,0:T(1,128)S(1)}, u32[]{:S(2)}, u32[]{:S(2)}) async-start(f32[8,256,1]{1,2,0:T(1,128)} %broadcast_in_dim.72), calls=%async_computation.2 | async-start | bytes 16384 | tf_op jit(solution)/shard_map/all_to_all | solution.py:27
  171.4 5.3 %copy-start.3 = (bf16[128,4096]{1,0:T(8,128)(2,1)S(1)}, bf16[128,4096]{1,0:T(8,128)(2,1)}, u32[]{:S(2)}) copy-start(bf16[128,4096]{1,0:T(8,128)(2,1)} %param.40) | copy-start | bytes 3145732
  171.4 5.3 %copy-start.10 = (f32[128]{0:T(128)S(1)}, f32[128]{0:T(128)}, u32[]{:S(2)}) copy-start(f32[128]{0:T(128)} %param.38) | copy-start | bytes 1540
  210.2 0.7 copy-start.5
Sparse Core Ops, SparseCore 0:
  9.2 28.2 all-gather.2
  45.6 88.9 all-gather.4
where the time goes:
time: 220 us; the launch traced here: 219 us
  waiting for transfers between devices  93.3 us (42%)
  blocking collectives  30.5 us (14%)
  matrix products  28.8 us (13%)
  local copies, waits for them, and re-layouts  22.8 us (10%)
  starting transfers between devices  21.3 us (10%)
  between operations  14.5 us (7%)
  other arithmetic  6.97 us (3%)
    all_gather x1, waiting for transfers between devices, in_one_piece(): out = lax.all_gather(both, axis, axis=dim, tiled=True)  49.2 us
    all_to_all x1, blocking collectives, sum_at_owner(): lax.all_to_all(in_blocks(shard, dim, count), axis, 0, 0, tiled=True)  30.5 us
    all_gather x1, waiting for transfers between devices, shards(): lax.all_gather(tokens, 'tp', axis=1, tiled=True).astype(jnp.float32)  30.1 us
    all_to_all x3, starting transfers between devices, from_everyone(): return lax.all_to_all(copies, axis, split_axis=0, concat_axis=0, tiled=True)  18.2 us
    all_to_all x3, waiting for transfers between devices, from_everyone(): return lax.all_to_all(copies, axis, split_axis=0, concat_axis=0, tiled=True)  11.9 us
    dot_general x5, matrix products, accumulate(): return jnp.dot(source, weight, preferred_element_type=jnp.float32)  10.7 us
    unnamed x35, local copies, waits for them, and re-layouts  8.57 us
    split x3, local copies, waits for them, and re-layouts, in_one_piece(): jnp.split(out, [sum(widths[:k]) for k in range(1, len(widths))], axis=along)  5.93 us
  transfers between devices with their start and end apart: 6, of which 6 were waited for; matrix products, arithmetic and copies ran while one was open for 6% of the time, Pallas kernels for 0%

commit v1 on v0

v1 whole, which is shorter than its diff:
```python
import functools
import math

import jax
import jax.numpy as jnp
from jax import lax
from jax.experimental import pallas as pl
from jax.experimental.pallas import tpu as pltpu
from jax.sharding import PartitionSpec as P

NOPE = 128
ROPE = 64
VDIM = 128
EPS = 1e-06
RATE_C = 8.0
THETA = 10000.0
NY, NX, NZ = 4, 4, 8
MESH = pl.DeviceIdType.MESH
F32, BF16 = jnp.float32, jnp.bfloat16
VM = pl.BlockSpec(memory_space=pltpu.VMEM)
ANY = pl.BlockSpec(memory_space=pl.ANY)


def remote(src, dst, send, recv, where):
    return pltpu.make_async_remote_copy(
        src_ref=src, dst_ref=dst, send_sem=send, recv_sem=recv, device_id=where, device_id_type=MESH
    )


def greet(partners):
    barrier = pltpu.get_barrier_semaphore()
    for where in partners:
        pl.semaphore_signal(barrier, inc=1, device_id=where, device_id_type=MESH)
    pl.semaphore_wait(barrier, len(partners))


def mm(a, b):
    return jnp.dot(a, b, preferred_element_type=F32)


def kernel_a(
    tok_ref, gain_ref, w_in, w_gate, w_q, w_lat, w_rope, lat_gain, w_exp, cos_ref, sin_ref,
    q_out, kv_out, rec_out, gate_out,
    tok, v_ig, v_q, v_lat, v_rope, v_exp, a_ig, a_q, a_lat, a_rope, sq,
    wsem, ssem, rsem,
):
    tp = lax.axis_index("tp")
    y, c = tp // 2, tp % 2
    sib = y * 2 + 1 - c
    up = ((y + 1) % NY) * 2 + c
    dn = ((y + 3) % NY) * 2 + c
    far = ((y + 2) % NY) * 2 + c
    rows = tok_ref.shape[0]
    half = rows // 2
    depth = tok_ref.shape[1]
    model = depth * 2 * NY

    loads = [
        pltpu.make_async_copy(w_in, v_ig.at[:, pl.ds(0, 128)], wsem.at[0]),
        pltpu.make_async_copy(w_gate, v_ig.at[:, pl.ds(128, 128)], wsem.at[1]),
        pltpu.make_async_copy(w_q, v_q, wsem.at[2]),
        pltpu.make_async_copy(w_lat, v_lat, wsem.at[3]),
        pltpu.make_async_copy(w_rope, v_rope, wsem.at[4]),
        pltpu.make_async_copy(w_exp, v_exp, wsem.at[5]),
    ]
    for load in loads:
        load.start()
    greet([{"tp": sib}, {"tp": up}, {"tp": dn}])

    h0, h1 = pl.ds(0, half), pl.ds(half, half)

    def msg(k, src, slot, part, where):
        return remote(src, tok.at[slot, part], ssem.at[k], rsem.at[k], {"tp": where})

    sent = []

    def send(k, src, slot, part, where):
        copy = msg(k, src, slot, part, where)
        copy.start()
        sent.append(copy)

    def arrived(k, slot, part):
        msg(k, tok.at[slot, part], slot, part, sib).wait_recv()

    def own(part):
        return tok_ref.at[part]

    send(1, own(h0), tp, h0, up)
    send(3, own(h1), tp, h1, dn)
    send(0, tok_ref, tp, pl.ds(0, rows), sib)
    send(2, own(h1), tp, h1, up)
    send(4, own(h0), tp, h0, dn)

    def chunk(block, source, first):
        wide = block.astype(F32)
        square = wide * wide
        folded = square[:, 0:128]
        for k in range(1, depth // 128):
            folded = folded + square[:, k * 128 : (k + 1) * 128]
        at = pl.ds(pl.multiple_of(source * depth, depth), depth)
        low = (wide * gain_ref[:, at]).astype(BF16)
        parts = ((a_ig, v_ig), (a_q, v_q), (a_lat, v_lat), (a_rope, v_rope))
        if first:
            sq[...] = folded
            for acc, weight in parts:
                acc[...] = mm(low, weight[at, :])
        else:
            sq[...] += folded
            for acc, weight in parts:
                acc[...] += mm(low, weight[at, :])

    for load in loads[:5]:
        load.wait()
    chunk(tok_ref[...], tp, True)
    arrived(0, sib, pl.ds(0, rows))
    chunk(tok[sib], sib, False)

    arrived(1, dn, h0)
    send(5, tok.at[dn, h0], dn, h0, up)
    send(7, tok.at[dn, h0], dn, h0, sib)
    arrived(3, up, h1)
    send(6, tok.at[up, h1], up, h1, dn)
    send(9, tok.at[up, h1], up, h1, sib)
    arrived(2, dn, h1)
    send(8, tok.at[dn, h1], dn, h1, sib)
    arrived(4, up, h0)
    send(10, tok.at[up, h0], up, h0, sib)
    chunk(tok[dn], dn, False)
    chunk(tok[up], up, False)
    dn_sib = ((y + 3) % NY) * 2 + 1 - c
    up_sib = ((y + 1) % NY) * 2 + 1 - c
    far_sib = ((y + 2) % NY) * 2 + 1 - c
    arrived(7, dn_sib, h0)
    arrived(8, dn_sib, h1)
    chunk(tok[dn_sib], dn_sib, False)
    arrived(9, up_sib, h1)
    arrived(10, up_sib, h0)
    chunk(tok[up_sib], up_sib, False)
    arrived(5, far, h0)
    send(11, tok.at[far, h0], far, h0, sib)
    arrived(6, far, h1)
    send(12, tok.at[far, h1], far, h1, sib)
    chunk(tok[far], far, False)
    arrived(11, far_sib, h0)
    arrived(12, far_sib, h1)
    chunk(tok[far_sib], far_sib, False)
    loads[5].wait()

    inverse = lax.rsqrt(jnp.sum(sq[...], axis=1, keepdims=True) / model + EPS)
    latent = inverse * a_lat[...]
    spread = lax.rsqrt(jnp.mean(latent * latent, axis=1, keepdims=True) + EPS)
    latent = (latent * spread * lat_gain[...]).astype(BF16)
    expanded = mm(latent, v_exp[...]).T
    kv_out[0:NOPE, :] = expanded[0:NOPE].astype(BF16)
    kv_out[NOPE + ROPE :, :] = expanded[NOPE:].astype(BF16)
    query = inverse * a_q[...]
    turned = jnp.concatenate([query[:, NOPE:], inverse * a_rope[...]], axis=1).T
    cosine, sine = cos_ref[...], sin_ref[...]
    hr = ROPE // 2
    u, w = turned[0:hr], turned[hr:ROPE]
    q_out[0:NOPE, :] = query[:, 0:NOPE].T.astype(BF16)
    q_out[NOPE : NOPE + hr, :] = (u * cosine - w * sine).astype(BF16)
    q_out[NOPE + hr :, :] = (w * cosine + u * sine).astype(BF16)
    u, w = turned[ROPE : ROPE + hr], turned[ROPE + hr :]
    kv_out[NOPE : NOPE + hr, :] = (u * cosine - w * sine).astype(BF16)
    kv_out[NOPE + hr : NOPE + ROPE, :] = (w * cosine + u * sine).astype(BF16)
    ig = inverse * a_ig[...]
    rec_out[...] = ig[:, 0:128].astype(BF16)
    gate_out[...] = ig[:, 128:256]
    for copy in sent:
        copy.wait_send()


def call_a(tokens, pre_gain, w_in, w_gate, w_q, w_lat, w_rope, lat_gain, w_exp, cosine, sine):
    rows, depth = tokens.shape
    model = w_in.shape[0]
    return pl.pallas_call(
        kernel_a,
        name="gather_project",
        out_shape=(
            jax.ShapeDtypeStruct((NOPE + ROPE, rows), BF16),
            jax.ShapeDtypeStruct((NOPE + ROPE + VDIM, rows), BF16),
            jax.ShapeDtypeStruct((rows, 128), BF16),
            jax.ShapeDtypeStruct((rows, 128), F32),
        ),
        in_specs=[VM, VM, ANY, ANY, ANY, ANY, ANY, VM, ANY, VM, VM],
        out_specs=(VM, VM, VM, VM),
        scratch_shapes=[
            pltpu.VMEM((2 * NY, rows, depth), BF16),
            pltpu.VMEM((model, 256), BF16),
            pltpu.VMEM((model, NOPE + ROPE), BF16),
            pltpu.VMEM((model, 512), BF16),
            pltpu.VMEM((model, ROPE), BF16),
            pltpu.VMEM((512, NOPE + VDIM), BF16),
            pltpu.VMEM((rows, 256), F32),
            pltpu.VMEM((rows, NOPE + ROPE), F32),
            pltpu.VMEM((rows, 512), F32),
            pltpu.VMEM((rows, ROPE), F32),
            pltpu.VMEM((rows, 128), F32),
            pltpu.SemaphoreType.DMA((6,)),
            pltpu.SemaphoreType.DMA((13,)),
            pltpu.SemaphoreType.DMA((13,)),
        ],
        compiler_params=pltpu.CompilerParams(
            collective_id=0, has_side_effects=True, vmem_limit_bytes=48 * 1024 * 1024
        ),
    )(tokens, pre_gain, w_in, w_gate, w_q, w_lat, w_rope, lat_gain, w_exp, cosine, sine)


def shifted(values, by, fill):
    row = lax.broadcasted_iota(jnp.int32, values.shape, 0)
    return jnp.where(row < by, fill, pltpu.roll(values, by, 0))


def minus_expm1(x):
    series = 1.0 + x * (1.0 / 7.0)
    for n in (6.0, 5.0, 4.0, 3.0, 2.0):
        series = 1.0 + (x * (1.0 / n)) * series
    return jnp.where(x > -0.25, -x * series, 1.0 - jnp.exp(x))


def softplus(x):
    small = jnp.exp(-jnp.abs(x))
    t = small / (2.0 + small)
    t2 = t * t
    series = 1.0 / 17.0
    for n in (15.0, 13.0, 11.0, 9.0, 7.0, 5.0, 3.0, 1.0):
        series = 1.0 / n + t2 * series
    return jnp.maximum(x, 0.0) + 2.0 * t * series


def kernel_b(
    q_ref, kv_ref, rec_ref, gate_ref, rf_ref, taps_ref, rmap_ref, imap_ref, decay_ref,
    rec_t, att_t, sums,
    kv, kn, qs, halo, ext, m_s, l_s, o_s, cum_s, loc_s, cx, cz, mine_x, mine_z, po, ps, go, gs,
    kss, krs, qss, qrs, hsem, xss, xrs, zss, zrs, oss, ors, tss, trs,
):
    sp = lax.axis_index("sp")
    z, x = sp // NX, sp % NX
    keys = q_ref.shape[1]

    def at_zx(zz, xx):
        return {"sp": zz * NX + xx}

    zup, zdn = (z + 1) % NZ, (z + NZ - 1) % NZ
    succ = (sp + 1) % (NX * NZ)
    pred = (sp + NX * NZ - 1) % (NX * NZ)
    xs_other = [(x + d) % NX for d in range(1, NX)]
    zs_other = [(z + d) % NZ for d in range(1, NZ)]
    greet(
        [at_zx(z, xx) for xx in xs_other]
        + [at_zx(zz, x) for zz in zs_other]
        + [{"sp": succ}, {"sp": pred}]
    )
    sent = []

    def go_send(copy):
        copy.start()
        sent.append(copy)

    kpart, vpart = pl.ds(0, NOPE + ROPE), pl.ds(NOPE + ROPE, VDIM)
    parts = (kpart, vpart)

    def kv_msg(src, slot, part, k, where_z):
        return remote(src, kv.at[slot, parts[part]], kss.at[k], krs.at[k], at_zx(where_z, x))

    def kid(direction, hop, part):
        return direction * 8 + (hop - 1) * 2 + part

    go_send(kv_msg(kv_ref.at[kpart], z, 0, kid(0, 1, 0), zup))
    go_send(kv_msg(kv_ref.at[kpart], z, 0, kid(1, 1, 0), zdn))
    go_send(kv_msg(kv_ref.at[vpart], z, 1, kid(0, 1, 1), zup))
    go_send(kv_msg(kv_ref.at[vpart], z, 1, kid(1, 1, 1), zdn))
    tail = rec_ref.shape[0] - 16
    go_send(remote(rec_ref.at[pl.ds(tail, 16)], halo, hsem.at[0], hsem.at[1], {"sp": succ}))
    for d in range(1, NX):
        go_send(remote(q_ref, qs.at[x], qss.at[d - 1], qrs.at[d - 1], at_zx(z, (x + d) % NX)))

    scale = math.log2(math.e) / math.sqrt(NOPE + ROPE)
    low = -1e30

    def begin(slot):
        m_s[slot] = jnp.full((1, keys), low, F32)
        l_s[slot] = jnp.zeros((1, keys), F32)
        o_s[slot] = jnp.zeros((VDIM, keys), F32)

    for xx in range(NX):
        begin(xx)

    def attend(slot, queries, values, masked):
        scores = mm(kn[...], queries) * scale
        if masked:
            key = lax.broadcasted_iota(jnp.int32, scores.shape, 0)
            place = lax.broadcasted_iota(jnp.int32, scores.shape, 1)
            scores = jnp.where(key <= place, scores, low)
        before = m_s[slot]
        largest = jnp.maximum(before, jnp.max(scores, axis=0, keepdims=True))
        weights = jnp.exp2(scores - largest)
        shrink = jnp.exp2(before - largest)
        m_s[slot] = largest
        l_s[slot] = l_s[slot] * shrink + jnp.sum(weights, axis=0, keepdims=True)
        o_s[slot] = o_s[slot] * shrink + mm(values, weights.astype(BF16))

    kn[...] = kv_ref[kpart, :].T
    attend(x, q_ref[...], kv_ref[vpart, :], True)

    remote(halo, halo, hsem.at[0], hsem.at[1], {"sp": succ}).wait_recv()
    first = sp == 0
    rows = rec_ref.shape[0]
    ext[0:16, :] = jnp.where(first, 0.0, halo[...].astype(F32))
    ext[16:, :] = rec_ref[...].astype(F32)
    convolved = taps_ref[0:1, :] * ext[13 : 13 + rows, :]
    for k in range(1, 4):
        convolved = convolved + taps_ref[k : k + 1, :] * ext[13 + k : 13 + k + rows, :]
    conv_low = convolved.astype(BF16)
    rate = jax.nn.sigmoid(mm(conv_low, rmap_ref[...]))
    entry = jax.nn.sigmoid(mm(conv_low, imap_ref[...]))
    factor = jnp.broadcast_to(rf_ref[...], (128, rows)).T
    log_keep = (-RATE_C) * factor * rate * softplus(-decay_ref[...])
    cum = jnp.exp(log_keep)
    local = jnp.sqrt(minus_expm1(2.0 * log_keep)) * entry * convolved
    step = 1
    while step < rows:
        local = local + cum * shifted(local, step, 0.0)
        cum = cum * shifted(cum, step, 1.0)
        step *= 2
    cum_s[...] = cum
    loc_s[...] = local
    mine_x[0:1, :] = cum[rows - 1 :]
    mine_x[1:2, :] = local[rows - 1 :]
    for d in range(1, NX):
        go_send(remote(mine_x, cx.at[x], xss.at[d - 1], xrs.at[d - 1], at_zx(z, (x + d) % NX)))

    def got(slot, part, k):
        kv_msg(kv.at[slot, parts[part]], slot, part, k, zup).wait_recv()

    def take_hop(hop):
        below, above = (z + NZ - hop) % NZ, (z + hop) % NZ
        for part in (0, 1):
            for direction, slot, to in ((0, below, zup), (1, above, zdn)):
                if hop == 4 and direction != part:
                    continue
                got(slot, part, kid(direction, hop, part))
                if hop < 3 or (hop == 3 and direction == part):
                    go_send(kv_msg(kv.at[slot, parts[part]], slot, part, kid(direction, hop + 1, part), to))
        return below, above

    def against(slot):
        kn[...] = kv[slot, 0 : NOPE + ROPE, :].T

        def one(i, carry):
            xx = (x + i) % NX
            attend(xx, qs[xx], kv[slot, NOPE + ROPE :, :], False)
            return carry

        lax.fori_loop(0, NX, one, 0)

    def hop_work(hop):
        below, above = take_hop(hop)
        return below, above

    qs[x] = q_ref[...]
    for d in range(1, NX):
        remote(q_ref, qs.at[(x + NX - d) % NX], qss.at[d - 1], qrs.at[d - 1], at_zx(z, x)).wait_recv()
    for d in range(1, NX):

        @pl.when(x + d < NX)
        def _():
            attend(x + d, qs[jnp.minimum(x + d, NX - 1)], kv_ref[vpart, :], False)

    for hop in range(1, 5):
        below, above = take_hop(hop)

        @pl.when(below < z)
        def _():
            against(below)

        if hop < 4:

            @pl.when(above < z)
            def _():
                against(above)

        if hop == 1:
            cx[x] = mine_x[...]
            for d in range(1, NX):
                remote(mine_x, cx.at[(x + NX - d) % NX], xss.at[d - 1], xrs.at[d - 1], at_zx(z, x)).wait_recv()
            pa, pb = jnp.ones((1, 128), F32), jnp.zeros((1, 128), F32)
            ta, tb = pa, pb
            for i in range(NX):
                a, b = cx[i, 0:1, :], cx[i, 1:2, :]
                ta, tb = ta * a, a * tb + b
                pa = jnp.where(i < x, pa * a, pa)
                pb = jnp.where(i < x, a * pb + b, pb)
            mine_z[0:1, :] = ta
            mine_z[1:2, :] = tb
            for d in range(1, NZ):
                go_send(remote(mine_z, cz.at[z], zss.at[d - 1], zrs.at[d - 1], at_zx((z + d) % NZ, x)))
        if hop == 3:
            cz[z] = mine_z[...]
            for d in range(1, NZ):
                remote(mine_z, cz.at[(z + NZ - d) % NZ], zss.at[d - 1], zrs.at[d - 1], at_zx(z, x)).wait_recv()
            entering = jnp.zeros((1, 128), F32)
            for i in range(NZ):
                entering = jnp.where(i < z, cz[i, 0:1, :] * entering + cz[i, 1:2, :], entering)
            entering = pa * entering + pb
            state = loc_s[...] + cum_s[...] * entering
            turned = (state * jax.nn.gelu(gate_ref[...])).T
            rec_t[...] = turned
            sums[0:1, :] = jnp.sum(turned * turned, axis=0, keepdims=True)

    for d in range(1, NX):
        xx = (x + d) % NX
        total = l_s[xx]
        po[d - 1] = (o_s[xx] / jnp.where(total > 0.0, total, 1.0)).astype(BF16)
        ps[d - 1, 0:1, :] = m_s[xx]
        ps[d - 1, 1:2, :] = total
        go_send(remote(po.at[d - 1], go.at[d - 1], oss.at[d - 1], ors.at[d - 1], at_zx(z, xx)))
        go_send(remote(ps.at[d - 1], gs.at[d - 1], tss.at[d - 1], trs.at[d - 1], at_zx(z, xx)))
    largest = m_s[x]
    for d in range(1, NX):
        remote(ps.at[d - 1], gs.at[d - 1], tss.at[d - 1], trs.at[d - 1], at_zx(z, x)).wait_recv()
        largest = jnp.maximum(largest, gs[d - 1, 0:1, :])
    share = jnp.exp2(m_s[x] - largest)
    total = l_s[x] * share
    out = o_s[x] * share
    for d in range(1, NX):
        remote(po.at[d - 1], go.at[d - 1], oss.at[d - 1], ors.at[d - 1], at_zx(z, x)).wait_recv()
        share = gs[d - 1, 1:2, :] * jnp.exp2(gs[d - 1, 0:1, :] - largest)
        total = total + share
        out = out + go[d - 1].astype(F32) * share
    out = out / total
    att_t[...] = out
    sums[1:2, :] = jnp.sum(out * out, axis=0, keepdims=True)
    for copy in sent:
        copy.wait_send()


def call_b(q, kv, rec, gate, rf, taps, rmap, imap, decay):
    keys = q.shape[1]
    dma = pltpu.SemaphoreType.DMA
    return pl.pallas_call(
        kernel_b,
        name="attend_recur",
        out_shape=(
            jax.ShapeDtypeStruct((128, keys), F32),
            jax.ShapeDtypeStruct((VDIM, keys), F32),
            jax.ShapeDtypeStruct((2, keys), F32),
        ),
        in_specs=[VM] * 9,
        out_specs=(VM, VM, VM),
        scratch_shapes=[
            pltpu.VMEM((NZ, NOPE + ROPE + VDIM, keys), BF16),
            pltpu.VMEM((keys, NOPE + ROPE), BF16),
            pltpu.VMEM((NX, NOPE + ROPE, keys), BF16),
            pltpu.VMEM((16, 128), BF16),
            pltpu.VMEM((16 + keys, 128), F32),
            pltpu.VMEM((NX, 1, keys), F32),
            pltpu.VMEM((NX, 1, keys), F32),
            pltpu.VMEM((NX, VDIM, keys), F32),
            pltpu.VMEM((keys, 128), F32),
            pltpu.VMEM((keys, 128), F32),
            pltpu.VMEM((NX, 2, 128), F32),
            pltpu.VMEM((NZ, 2, 128), F32),
            pltpu.VMEM((2, 128), F32),
            pltpu.VMEM((2, 128), F32),
            pltpu.VMEM((NX - 1, VDIM, keys), BF16),
            pltpu.VMEM((NX - 1, 2, keys), F32),
            pltpu.VMEM((NX - 1, VDIM, keys), BF16),
            pltpu.VMEM((NX - 1, 2, keys), F32),
            dma((16,)), dma((16,)),
            dma((NX - 1,)), dma((NX - 1,)),
            dma((2,)),
            dma((NX - 1,)), dma((NX - 1,)),
            dma((NZ - 1,)), dma((NZ - 1,)),
            dma((NX - 1,)), dma((NX - 1,)),
            dma((NX - 1,)), dma((NX - 1,)),
        ],
        compiler_params=pltpu.CompilerParams(
            collective_id=1, has_side_effects=True, vmem_limit_bytes=32 * 1024 * 1024
        ),
    )(q, kv, rec, gate, rf, taps, rmap, imap, decay)


def kernel_c(
    rec_t, att_t, sums, rgain, again, w_rec, w_att, post,
    out_ref,
    got_s, act, w, pair_out, pair_in, part, f_out, f_in, n_out, n_in,
    wsem, sss, srs, pss, prs, fss, frs, nss, nrs,
):
    tp = lax.axis_index("tp")
    y, c = tp // 2, tp % 2
    sib = y * 2 + 1 - c
    up = ((y + 1) % NY) * 2 + c
    dn = ((y + 3) % NY) * 2 + c
    model = w.shape[1]
    rows = out_ref.shape[0]
    half = model // 2
    loads = [
        pltpu.make_async_copy(w_rec, w.at[pl.ds(0, 128)], wsem.at[0]),
        pltpu.make_async_copy(w_att, w.at[pl.ds(128, 128)], wsem.at[1]),
    ]
    for load in loads:
        load.start()
    n = 2 * NY
    greet([{"tp": (tp + d) % n} for d in range(1, n)])
    sent = []

    def go_send(copy):
        copy.start()
        sent.append(copy)

    for d in range(1, n):
        go_send(remote(sums, got_s.at[d - 1], sss.at[d - 1], srs.at[d - 1], {"tp": (tp + d) % n}))
    total = sums[...]
    for d in range(1, n):
        remote(sums, got_s.at[d - 1], sss.at[d - 1], srs.at[d - 1], {"tp": sib}).wait_recv()
        total = total + got_s[d - 1]
    inverse = lax.rsqrt(total / (128 * n) + EPS)
    act[:, 0:128] = ((rec_t[...] * inverse[0:1, :]).T * rgain[...]).astype(BF16)
    act[:, 128:256] = ((att_t[...] * inverse[1:2, :]).T * again[...]).astype(BF16)
    for load in loads:
        load.wait()

    order = [(y + 2) % NY, (y + 1) % NY, (y + 3) % NY, y]
    for k, yy in enumerate(order):
        block = act[pl.ds(pl.multiple_of(yy * 2 * rows + (1 - c) * rows, rows), rows), :]
        pair_out[k] = mm(block, w[...]).astype(BF16)
        go_send(remote(pair_out.at[k], pair_in.at[k], pss.at[k], prs.at[k], {"tp": sib}))

    def chip_sum(k):
        yy = order[k]
        block = act[pl.ds(pl.multiple_of(yy * 2 * rows + c * rows, rows), rows), :]
        value = mm(block, w[...])
        remote(pair_out.at[k], pair_in.at[k], pss.at[k], prs.at[k], {"tp": sib}).wait_recv()
        return value + pair_in[k].astype(F32)

    f_out[...] = chip_sum(0).astype(BF16)
    left, right = pl.ds(0, half), pl.ds(half, half)
    go_send(remote(f_out.at[:, left], f_in.at[:, left], fss.at[0], frs.at[0], {"tp": up}))
    go_send(remote(f_out.at[:, right], f_in.at[:, right], fss.at[1], frs.at[1], {"tp": dn}))
    part[0] = chip_sum(1)
    n_out[0, :, half:] = part[0, :, half:].astype(BF16)
    go_send(remote(n_out.at[0, :, right], n_in.at[0, :, right], nss.at[0], nrs.at[0], {"tp": up}))
    part[1] = chip_sum(2)
    n_out[1, :, 0:half] = part[1, :, 0:half].astype(BF16)
    go_send(remote(n_out.at[1, :, left], n_in.at[1, :, left], nss.at[1], nrs.at[1], {"tp": dn}))
    own = chip_sum(3)
    remote(f_out.at[:, left], f_in.at[:, left], fss.at[0], frs.at[0], {"tp": up}).wait_recv()
    n_out[0, :, 0:half] = (part[0, :, 0:half] + f_in[:, 0:half].astype(F32)).astype(BF16)
    go_send(remote(n_out.at[0, :, left], n_in.at[0, :, left], nss.at[2], nrs.at[2], {"tp": up}))
    remote(f_out.at[:, right], f_in.at[:, right], fss.at[1], frs.at[1], {"tp": dn}).wait_recv()
    n_out[1, :, half:] = (part[1, :, half:] + f_in[:, half:].astype(F32)).astype(BF16)
    go_send(remote(n_out.at[1, :, right], n_in.at[1, :, right], nss.at[3], nrs.at[3], {"tp": dn}))
    part[0] = own
    for k, (side, cols) in enumerate(((0, right), (1, left), (0, left), (1, right))):
        remote(n_out.at[side, :, cols], n_in.at[side, :, cols], nss.at[k], nrs.at[k], {"tp": up}).wait_recv()
    mixed = part[0] + n_in[0].astype(F32) + n_in[1].astype(F32)
    spread = lax.rsqrt(jnp.mean(mixed * mixed, axis=1, keepdims=True) + EPS)
    out_ref[...] = (mixed * spread * post[...]).astype(BF16)
    for copy in sent:
        copy.wait_send()


def call_c(rec_t, att_t, sums, rgain, again, w_rec, w_att, post):
    keys = rec_t.shape[1]
    n = 2 * NY
    rows = keys // n
    model = w_rec.shape[1]
    dma = pltpu.SemaphoreType.DMA
    return pl.pallas_call(
        kernel_c,
        name="project_out",
        out_shape=jax.ShapeDtypeStruct((rows, model), BF16),
        in_specs=[VM, VM, VM, VM, VM, ANY, ANY, VM],
        out_specs=VM,
        scratch_shapes=[
            pltpu.VMEM((n - 1, 2, keys), F32),
            pltpu.VMEM((keys, 256), BF16),
            pltpu.VMEM((256, model), BF16),
            pltpu.VMEM((NY, rows, model), BF16),
            pltpu.VMEM((NY, rows, model), BF16),
            pltpu.VMEM((2, rows, model), F32),
            pltpu.VMEM((rows, model), BF16),
            pltpu.VMEM((rows, model), BF16),
            pltpu.VMEM((2, rows, model), BF16),
            pltpu.VMEM((2, rows, model), BF16),
            dma((2,)),
            dma((n - 1,)), dma((n - 1,)),
            dma((NY,)), dma((NY,)),
            dma((2,)), dma((2,)),
            dma((4,)), dma((4,)),
        ],
        compiler_params=pltpu.CompilerParams(
            collective_id=2, has_side_effects=True, vmem_limit_bytes=32 * 1024 * 1024
        ),
    )(rec_t, att_t, sums, rgain, again, w_rec, w_att, post)


def shards(
    tokens, pre_gain, rate_factor, w_rec_in, w_rec_gate, conv_taps, rate_maps, input_maps,
    decay_param, w_query, w_latent, w_rope_key, latent_gain, w_expand, rec_gain, att_gain,
    w_out_rec, w_out_att, post_gain,
):
    rows = tokens.shape[0]
    frequency = 1.0 / THETA ** (jnp.arange(0, ROPE, 2).astype(F32) / ROPE)
    places = (lax.axis_index("sp") * rows + jnp.arange(rows)).astype(F32)
    turned = places[None, :] * frequency[:, None]
    cosine, sine = jnp.cos(turned), jnp.sin(turned)
    q, kv, rec, gate = call_a(
        tokens, pre_gain[None], w_rec_in, w_rec_gate, w_query, w_latent, w_rope_key,
        latent_gain[None], w_expand, cosine, sine,
    )
    rec_t, att_t, sums = call_b(
        q, kv, rec, gate, rate_factor[None], conv_taps, rate_maps[0], input_maps[0], decay_param[None]
    )
    return call_c(
        rec_t, att_t, sums, rec_gain[None], att_gain[None], w_out_rec, w_out_att, post_gain[None]
    )


def solution(mesh):
    placed = (
        P("sp", "tp"), P(), P("sp"), P(None, "tp"), P(None, "tp"), P(None, "tp"),
        P("tp", None, None), P("tp", None, None), P("tp"), P(None, "tp"), P(), P(), P(),
        P(None, "tp"), P("tp"), P("tp"), P("tp", None), P("tp", None), P(),
    )
    return jax.shard_map(
        shards, mesh=mesh, in_specs=placed, out_specs=P(("sp", "tp"), None), check_vma=False
    )
```

time: 220 us -> 80.2 us (0.36)
  the two profiles are of different devices: /device:TPU:228 before, /device:TPU:1 now
where the time goes in v1:
time: 80.2 us; the launch traced here: 80.1 us
  Pallas kernels  72.3 us (90%)
  local copies, waits for them, and re-layouts  7.26 us (9%)
    pallas_call x1, Pallas kernels, call_b(): pl.pallas_call(kernel_b, name='attend_recur', out_shape=(jax.ShapeDtypeSt...  31 us
    pallas_call x1, Pallas kernels, call_c(): pl.pallas_call(kernel_c, name='project_out', out_shape=jax.ShapeDtypeStru...  23.6 us
    pallas_call x1, Pallas kernels, call_a(): pl.pallas_call(kernel_a, name='gather_project', out_shape=(jax.ShapeDtype...  17.7 us
    unnamed x35, local copies, waits for them, and re-layouts  7.26 us

profile of v1, /device:TPU:1, one launch (start us, length us, event | category | flops | bytes accessed | tf_op | source)
XLA Modules:
  0.0 80.1 jit_solution(6396542986259181405)
XLA Ops:
  0.0 0.2 multiply_sine_fusion
  0.2 1.5 %copy.21.w_rope = bf16[4096,64]{1,0:T(8,128)(2,1)S(1)} copy(bf16[4096,64]{0,1:T(8,128)(2,1)} %param.30) | data formatting | bytes 1048576 | tf_op args[11]
  1.7 0.0 copy-start.2
  1.8 0.0 copy-start.3
  1.8 0.0 copy-start.4
  1.8 0.0 copy-start.8
  1.8 0.0 copy-start.11
  1.8 4.0 %copy.20.w_q = bf16[4096,192]{1,0:T(8,128)(2,1)} copy(bf16[4096,192]{0,1:T(8,128)(2,1)} %param.28) | data formatting | bytes 3145728 | tf_op args[9]
  5.8 0.0 copy-done.2
  5.8 0.0 copy-done.3
  5.8 0.0 copy-done.8
  5.8 0.0 copy-done.11
  5.8 0.0 copy-start.5
  5.9 0.9 %copy-done.5 = bf16[512,256]{1,0:T(8,128)(2,1)S(1)} copy-done((bf16[512,256]{1,0:T(8,128)(2,1)S(1)}, bf16[512,256]{1,0:T(8,128)(2,1)}, u32[]{:S(2)}) %copy-start.5) | copy-done | bytes 262168
  6.8 0.0 copy-start.13
  6.8 0.0 copy-start
  6.8 0.0 copy-start.1
  6.8 0.0 copy-start.9
  6.9 0.0 copy-start.14
  6.9 0.0 copy-start.15
  6.9 17.7 %gather_project.1 = (bf16[192,256]{1,0:T(8,128)(2,1)S(1)}, bf16[320,256]{1,0:T(8,128)(2,1)S(1)}, bf16[256,128]{1,0:T(8,128)(2,1)S(1)}, f32[256,128]{1,0:T(8,128)S(1)}) custom-call(bf16[256,512]{1,0:T(8,128)(2,1)S(1)} %copy-done.4, f32[1,4096]{1,0:T(1,128)S(1)} %bitcast.11, bf16[4096,128]{1,0:T(8,128)(2,1)S(1)} %copy-done.2, bf16[4096,128]{1,0:T(8,128)(2,1)S(1)} %copy-done.3, ...), custom_call_target="tpu_custom_call" | custom-call | tf_op jit(solution)/shard_map/gather_project/pallas_call | solution.py:177
  24.7 31.0 %attend_recur.1 = (f32[128,256]{1,0:T(8,128)S(1)}, f32[128,256]{1,0:T(8,128)S(1)}, f32[2,256]{1,0:T(2,128)S(1)}) custom-call(bf16[192,256]{1,0:T(8,128)(2,1)S(1)} %get-tuple-element.12.q_ref, bf16[320,256]{1,0:T(8,128)(2,1)S(1)} %get-tuple-element.13.kv_ref, bf16[256,128]{1,0:T(8,128)(2,1)S(1)} %get-tuple-element.14.rec_ref, ...), custom_call_target="tpu_custom_call" | custom-call | tf_op jit(solution)/shard_map/attend_recur/pallas_call | solution.py:442
  55.7 23.6 %project_out.1 = bf16[32,4096]{1,0:T(8,128)(2,1)S(1)} custom-call(f32[128,256]{1,0:T(8,128)S(1)} %get-tuple-element.16.rec_t, f32[128,256]{1,0:T(8,128)S(1)} %get-tuple-element.17.att_t, f32[2,256]{1,0:T(2,128)S(1)} %get-tuple-element.18.sums, f32[1,128]{1,0:T(1,128)S(1)} %bitcast.16, f32[1,128]{1,0:T(1,128)S(1)} %bitcast.17, bf16[128,4096]{1,0:T(8,128)(2,1)S(1)} %copy-done, ...), custom_call_target="tpu_custom_call" | custom-call | tf_op jit(solution)/shard_map/project_out/pallas_call | solution.py:571
  79.3 0.7 copy.23
  (17 shorter events, 0.0 us)
Async XLA Ops:
  1.7 4.1 %copy-start.2 = (bf16[4096,128]{1,0:T(8,128)(2,1)S(1)}, bf16[4096,128]{1,0:T(8,128)(2,1)}, u32[]{:S(2)}) copy-start(bf16[4096,128]{1,0:T(8,128)(2,1)} %w_in.1) | copy-start | bytes 3145732
  1.8 4.1 %copy-start.3 = (bf16[4096,128]{1,0:T(8,128)(2,1)S(1)}, bf16[4096,128]{1,0:T(8,128)(2,1)}, u32[]{:S(2)}) copy-start(bf16[4096,128]{1,0:T(8,128)(2,1)} %w_gate.1) | copy-start | bytes 3145732
  1.8 4.0 %copy-start.4 = (bf16[256,512]{1,0:T(8,128)(2,1)S(1)}, bf16[256,512]{1,0:T(8,128)(2,1)}, u32[]{:S(2)}) copy-start(bf16[256,512]{1,0:T(8,128)(2,1)} %tok_ref.1) | copy-start | bytes 786436
  1.8 4.0 %copy-start.8 = (f32[4096]{0:T(1024)S(1)}, f32[4096]{0:T(1024)}, u32[]{:S(2)}) copy-start(f32[4096]{0:T(1024)} %param.20) | copy-start | bytes 49156
  1.8 4.0 %copy-start.11 = (f32[512]{0:T(512)S(1)}, f32[512]{0:T(512)}, u32[]{:S(2)}) copy-start(f32[512]{0:T(512)} %param.31) | copy-start | bytes 6148
  5.8 1.0 %copy-start.5 = (bf16[512,256]{1,0:T(8,128)(2,1)S(1)}, bf16[512,256]{1,0:T(8,128)(2,1)}, u32[]{:S(2)}) copy-start(bf16[512,256]{1,0:T(8,128)(2,1)} %w_exp.1) | copy-start | bytes 786436
  6.8 17.8 %copy-start.6 = (bf16[1,128,128]{2,1,0:T(8,128)(2,1)S(1)}, bf16[1,128,128]{2,1,0:T(8,128)(2,1)}, u32[]{:S(2)}) copy-start(bf16[1,128,128]{2,1,0:T(8,128)(2,1)} %param.25) | copy-start | bytes 98308
  6.8 17.8 %copy-start.7 = (bf16[1,128,128]{2,1,0:T(8,128)(2,1)S(1)}, bf16[1,128,128]{2,1,0:T(8,128)(2,1)}, u32[]{:S(2)}) copy-start(bf16[1,128,128]{2,1,0:T(8,128)(2,1)} %param.26) | copy-start | bytes 98308
  6.8 17.8 %copy-start.10 = (f32[4,128]{1,0:T(4,128)S(1)}, f32[4,128]{1,0:T(4,128)}, u32[]{:S(2)}) copy-start(f32[4,128]{1,0:T(4,128)} %taps_ref.1) | copy-start | bytes 6148
  6.8 17.8 %copy-start.12 = (f32[256]{0:T(256)S(1)}, f32[256]{0:T(256)}, u32[]{:S(2)}) copy-start(f32[256]{0:T(256)} %param.21) | copy-start | bytes 3076
  6.8 17.9 %copy-start.13 = (f32[128]{0:T(128)S(1)}, f32[128]{0:T(128)}, u32[]{:S(2)}) copy-start(f32[128]{0:T(128)} %param.27) | copy-start | bytes 1540
  6.8 48.9 %copy-start = (bf16[128,4096]{1,0:T(8,128)(2,1)S(1)}, bf16[128,4096]{1,0:T(8,128)(2,1)}, u32[]{:S(2)}) copy-start(bf16[128,4096]{1,0:T(8,128)(2,1)} %w_rec.1) | copy-start | bytes 3145732
  6.8 48.9 %copy-start.1 = (bf16[128,4096]{1,0:T(8,128)(2,1)S(1)}, bf16[128,4096]{1,0:T(8,128)(2,1)}, u32[]{:S(2)}) copy-start(bf16[128,4096]{1,0:T(8,128)(2,1)} %w_att.1) | copy-start | bytes 3145732
  6.8 48.9 %copy-start.9 = (f32[4096]{0:T(1024)S(1)}, f32[4096]{0:T(1024)}, u32[]{:S(2)}) copy-start(f32[4096]{0:T(1024)} %param.37) | copy-start | bytes 49156
  6.9 48.9 %copy-start.14 = (f32[128]{0:T(128)S(1)}, f32[128]{0:T(128)}, u32[]{:S(2)}) copy-start(f32[128]{0:T(128)} %param.33) | copy-start | bytes 1540
  6.9 48.9 %copy-start.15 = (f32[128]{0:T(128)S(1)}, f32[128]{0:T(128)}, u32[]{:S(2)}) copy-start(f32[128]{0:T(128)} %param.34) | copy-start | bytes 1540

commit v2 on v0

v2 whole, which is shorter than its diff:
```python
import math

import jax
import jax.numpy as jnp
from jax import lax
from jax.experimental import pallas as pl
from jax.experimental.pallas import tpu as pltpu
from jax.sharding import PartitionSpec as P

NOPE = 128
ROPE = 64
VDIM = 128
EPS = 1e-06
RATE_C = 8.0
THETA = 10000.0
NY, NX, NZ = 4, 4, 8
NT = 2 * NY
PIECES = 4
LOW = -1e30
MESH = pl.DeviceIdType.MESH
F32, BF16 = jnp.float32, jnp.bfloat16
QK = NOPE + ROPE


def remote(src, dst, send, recv, where):
    return pltpu.make_async_remote_copy(
        src_ref=src, dst_ref=dst, send_sem=send, recv_sem=recv, device_id=where, device_id_type=MESH
    )


def greet(partners):
    barrier = pltpu.get_barrier_semaphore()
    for where in partners:
        pl.semaphore_signal(barrier, inc=1, device_id=where, device_id_type=MESH)
    pl.semaphore_wait(barrier, len(partners))


def hello(sem, where):
    pl.semaphore_signal(sem, inc=1, device_id=where, device_id_type=MESH)


def mm(a, b):
    return jnp.dot(a, b, preferred_element_type=F32)


def mm_t(a, b):
    return lax.dot_general(a, b, (((1,), (1,)), ((), ())), preferred_element_type=F32)


def shifted(values, by, fill):
    row = lax.broadcasted_iota(jnp.int32, values.shape, 0)
    return jnp.where(row < by, fill, pltpu.roll(values, by, 0))


def minus_expm1(x):
    series = 1.0 + x * (1.0 / 7.0)
    for n in (6.0, 5.0, 4.0, 3.0, 2.0):
        series = 1.0 + (x * (1.0 / n)) * series
    return jnp.where(x > -0.25, -x * series, 1.0 - jnp.exp(x))


def softplus(x):
    small = jnp.exp(-jnp.abs(x))
    t = small / (2.0 + small)
    t2 = t * t
    series = 1.0 / 17.0
    for n in (15.0, 13.0, 11.0, 9.0, 7.0, 5.0, 3.0, 1.0):
        series = 1.0 / n + t2 * series
    return jnp.maximum(x, 0.0) + 2.0 * t * series


LOADS = (
    "tok", "gain", "w_in", "w_gate", "w_q", "w_rope", "w_lat", "w_exp", "lat_gain", "cos", "sin",
    "rf", "taps", "rmap", "imap", "decay", "rgain", "again", "w_rec", "w_att", "post",
)


def layer(*refs):
    n_in = len(LOADS)
    src = dict(zip(LOADS, refs[:n_in]))
    out_ref = refs[n_in]
    (
        tok, gain, v_ig, v_qr, v_lat, v_exp, lat_gain, cos_s, sin_s, rf, taps, rmap, imap, decay,
        rgain, again, w_rec, w_att, post,
        a_ig, a_qr, a_lat, sq,
        own_kv, own_q, rec_s, gate_s, kv, qs, halo, ext, m_s, l_s, o_s, cum_s, loc_s,
        mine_x, cx, mine_z, cz, po, ps, go, gs,
        act_r, act_t, sums, got_s, inv_s, r_out, r_in, r_own, t_out, t_in, t_own,
        part, f_out, f_in, n_out, n_in_s,
        lsem, hi, ass, ars, kss, krs, qss, qrs, hsem, xss, xrs, zss, zrs, oss, ors, tss, trs,
        sss, srs, rss, rrs, pss, prs, fss, frs, nss, nrs,
    ) = refs[n_in + 1 :]

    sp, tp = lax.axis_index("sp"), lax.axis_index("tp")
    z, x = sp // NX, sp % NX
    y, c = tp // 2, tp % 2

    def at_tp(yy, cc):
        return yy * 2 + cc

    sib = at_tp(y, 1 - c)
    up, dn, far = (at_tp((y + d) % NY, c) for d in (1, 3, 2))
    up_sib, dn_sib, far_sib = (at_tp((y + d) % NY, 1 - c) for d in (1, 3, 2))

    def at_zx(zz, xx):
        return {"sp": zz * NX + xx}

    zup, zdn = at_zx((z + 1) % NZ, x), at_zx((z + NZ - 1) % NZ, x)
    xs = {d: at_zx(z, (x + d) % NX) for d in range(1, NX)}

    rows, depth = tok.shape[1], tok.shape[2]
    model = depth * NT
    half = rows // 2

    where = {
        "tok": tok.at[tp], "gain": gain, "w_in": v_ig.at[:, pl.ds(0, 128)],
        "w_gate": v_ig.at[:, pl.ds(128, 128)], "w_q": v_qr.at[pl.ds(0, QK)],
        "w_rope": v_qr.at[pl.ds(QK, ROPE)], "w_lat": v_lat, "w_exp": v_exp, "lat_gain": lat_gain,
        "cos": cos_s, "sin": sin_s, "rf": rf, "taps": taps, "rmap": rmap, "imap": imap,
        "decay": decay, "rgain": rgain, "again": again, "w_rec": w_rec, "w_att": w_att, "post": post,
    }
    load = {
        name: pltpu.make_async_copy(src[name], where[name], lsem.at[k])
        for k, name in enumerate(LOADS)
    }
    for name in LOADS:
        load[name].start()
    greet([{"tp": sib}, {"tp": up}, {"tp": dn}, xs[1], xs[3], zup, zdn])
    hello(hi.at[0], xs[3])
    hello(hi.at[1], {"tp": dn})
    hello(hi.at[2], {"tp": sib})

    sent = []

    def go_send(copy):
        copy.start()
        sent.append(copy)

    h0, h1, whole = pl.ds(0, half), pl.ds(half, half), pl.ds(0, rows)

    def tok_msg(k, slot, piece, to):
        at = tok.at[slot, piece]
        return remote(at, at, ass.at[k], ars.at[k], {"tp": to})

    def send(k, slot, piece, to):
        go_send(tok_msg(k, slot, piece, to))

    def arrived(k, slot, piece):
        tok_msg(k, slot, piece, sib).wait_recv()

    load["tok"].wait()
    send(1, tp, h0, up)
    send(3, tp, h1, dn)
    send(0, tp, whole, sib)
    send(2, tp, h1, up)
    send(4, tp, h0, dn)

    def chunk(source, first=False):
        wide = tok[source].astype(F32)
        square = wide * wide
        folded = square[:, 0:128]
        for k in range(1, depth // 128):
            folded = folded + square[:, k * 128 : (k + 1) * 128]
        at = pl.ds(pl.multiple_of(source * depth, depth), depth)
        low = (wide * gain[:, at]).astype(BF16)
        ig, qr, lat = mm(low, v_ig[at, :]), mm_t(low, v_qr[:, at]), mm(low, v_lat[at, :])
        if first:
            sq[...], a_ig[...], a_qr[...], a_lat[...] = folded, ig, qr, lat
        else:
            sq[...] += folded
            a_ig[...] += ig
            a_qr[...] += qr
            a_lat[...] += lat

    for name in ("gain", "w_in", "w_gate", "w_q", "w_rope", "w_lat"):
        load[name].wait()
    chunk(tp, True)
    pl.semaphore_wait(hi.at[2], 1)
    hello(hi.at[3], {"tp": dn})
    arrived(0, sib, whole)
    chunk(sib)
    arrived(1, dn, h0)
    send(5, dn, h0, up)
    send(7, dn, h0, sib)
    arrived(3, up, h1)
    send(6, up, h1, dn)
    send(9, up, h1, sib)
    arrived(2, dn, h1)
    send(8, dn, h1, sib)
    arrived(4, up, h0)
    send(10, up, h0, sib)
    chunk(dn)
    chunk(up)
    arrived(7, dn_sib, h0)
    arrived(8, dn_sib, h1)
    chunk(dn_sib)
    arrived(9, up_sib, h1)
    arrived(10, up_sib, h0)
    chunk(up_sib)
    arrived(5, far, h0)
    send(11, far, h0, sib)
    arrived(6, far, h1)
    send(12, far, h1, sib)
    chunk(far)
    for name in LOADS[7:]:
        load[name].wait()
    arrived(11, far_sib, h0)
    arrived(12, far_sib, h1)
    chunk(far_sib)

    inverse = lax.rsqrt(jnp.sum(sq[...], axis=1, keepdims=True) / model + EPS)
    latent = inverse * a_lat[...]
    spread = lax.rsqrt(jnp.mean(latent * latent, axis=1, keepdims=True) + EPS)
    latent = (latent * spread * lat_gain[...]).astype(BF16)
    expanded = mm(latent, v_exp[...]).T
    turned = (inverse * a_qr[:, NOPE:]).T
    cosine, sine = cos_s[...], sin_s[...]
    hr = ROPE // 2
    u, w = turned[ROPE : ROPE + hr], turned[ROPE + hr :]
    own_kv[0:NOPE, :] = expanded[0:NOPE].astype(BF16)
    own_kv[NOPE : NOPE + hr, :] = (u * cosine - w * sine).astype(BF16)
    own_kv[NOPE + hr : QK, :] = (w * cosine + u * sine).astype(BF16)
    own_kv[QK:, :] = expanded[NOPE:].astype(BF16)

    size = (QK + VDIM) // PIECES

    def piece_at(p):
        return pl.ds(p * size, size)

    def kv_msg(source, direction, hop, p):
        k = (direction * 4 + hop - 1) * PIECES + p
        slot = (z + (NZ - hop + 1 if direction == 0 else hop - 1)) % NZ
        return remote(
            source, kv.at[slot, piece_at(p)], kss.at[k], krs.at[k], zup if direction == 0 else zdn
        )

    def kv_goes(direction, hop, p):
        return hop < 4 or (hop == 4 and (direction == 0) == (p < PIECES // 2))

    for p in range(PIECES):
        for direction in (0, 1):
            go_send(kv_msg(own_kv.at[piece_at(p)], direction, 1, p))

    u, w = turned[0:hr], turned[hr:ROPE]
    own_q[0:NOPE, :] = (inverse * a_qr[:, 0:NOPE]).T.astype(BF16)
    own_q[NOPE : NOPE + hr, :] = (u * cosine - w * sine).astype(BF16)
    own_q[NOPE + hr :, :] = (w * cosine + u * sine).astype(BF16)
    rec_s[...] = (inverse * a_ig[:, 0:128]).astype(BF16)
    gate_s[...] = inverse * a_ig[:, 128:256]
    succ = {"sp": (sp + 1) % (NX * NZ)}
    tail = rows - 16

    pl.semaphore_wait(hi.at[0], 1)
    pl.semaphore_wait(hi.at[1], 1)

    def q_msg(d, slot):
        return remote(own_q, qs.at[slot], qss.at[d - 1], qrs.at[d - 1], xs[d])

    for d in (2, 1, 3):
        go_send(q_msg(d, x))

    for xx in range(NX):
        m_s[xx] = jnp.full((1, rows), LOW, F32)
        l_s[xx] = jnp.zeros((1, rows), F32)
        o_s[xx] = jnp.zeros((VDIM, rows), F32)

    scale = math.log2(math.e) / math.sqrt(QK)

    def attend(slots, queries, keys, values, masked):
        scores = [mm(keys, query) * scale for query in queries]
        if masked:
            key = lax.broadcasted_iota(jnp.int32, scores[0].shape, 0)
            place = lax.broadcasted_iota(jnp.int32, scores[0].shape, 1)
            scores = [jnp.where(key <= place, s, LOW) for s in scores]
        before = [m_s[k] for k in slots]
        most = [jnp.maximum(b, jnp.max(s, axis=0, keepdims=True)) for b, s in zip(before, scores)]
        weights = [jnp.exp2(s - m) for s, m in zip(scores, most)]
        shrink = [jnp.exp2(b - m) for b, m in zip(before, most)]
        for k, m, s, wt in zip(slots, most, shrink, weights):
            m_s[k] = m
            l_s[k] = l_s[k] * s + jnp.sum(wt, axis=0, keepdims=True)
        for k, s, wt in zip(slots, shrink, weights):
            o_s[k] = o_s[k] * s + mm(values, wt.astype(BF16))

    def unit(slot):
        attend(
            range(NX), [qs[k] for k in range(NX)], kv[slot, 0:QK, :].T, kv[slot, QK:, :], False
        )

    def poll(hop, pieces):
        for p in pieces:
            for direction in (0, 1):
                if kv_goes(direction, hop, p):
                    slot = (z + (NZ - hop if direction == 0 else hop)) % NZ
                    here = kv.at[slot, piece_at(p)]
                    k = (direction * 4 + hop - 1) * PIECES + p
                    remote(here, here, kss.at[k], krs.at[k], zup).wait_recv()
                    if kv_goes(direction, hop + 1, p):
                        go_send(kv_msg(here, direction, hop + 1, p))

    first_half, second_half = (0, 1), (2, 3)

    ext[16:, :] = rec_s[...].astype(F32)
    mine_tail = remote(rec_s.at[pl.ds(tail, 16)], halo, hsem.at[0], hsem.at[1], succ)
    go_send(mine_tail)
    own_k = own_kv[0:QK, :].T
    attend((x,), [own_q[...]], own_k, own_kv[QK:, :], True)
    poll(1, first_half)
    mine_tail.wait_recv()
    ext[0:16, :] = jnp.where(sp == 0, 0.0, halo[...].astype(F32))
    convolved = taps[0:1, :] * ext[13 : 13 + rows, :]
    for k in range(1, 4):
        convolved = convolved + taps[k : k + 1, :] * ext[13 + k : 13 + k + rows, :]
    conv_low = convolved.astype(BF16)
    rate = jax.nn.sigmoid(mm(conv_low, rmap[...]))
    entry = jax.nn.sigmoid(mm(conv_low, imap[...]))
    factor = jnp.broadcast_to(rf[...], (128, rows)).T
    log_keep = (-RATE_C) * factor * rate * softplus(-decay[...])
    cum = jnp.exp(log_keep)
    local = jnp.sqrt(minus_expm1(2.0 * log_keep)) * entry * convolved
    step = 1
    while step < rows:
        local = local + cum * shifted(local, step, 0.0)
        cum = cum * shifted(cum, step, 1.0)
        step *= 2
    cum_s[...] = cum
    loc_s[...] = local
    mine_x[0:1, :] = cum[rows - 1 :]
    mine_x[1:2, :] = local[rows - 1 :]

    def x_msg(d, slot):
        return remote(mine_x, cx.at[slot], xss.at[d - 1], xrs.at[d - 1], xs[d])

    for d in range(1, NX):
        go_send(x_msg(d, x))
    poll(1, second_half)

    qs[x] = own_q[...]
    for d in range(1, NX):
        q_msg(d, (x + NX - d) % NX).wait_recv()
    for xx in range(1, NX):

        @pl.when(x < xx)
        def _():
            attend((xx,), [qs[xx]], own_kv[0:QK, :].T, own_kv[QK:, :], False)

    def against(slot):
        @pl.when(slot < z)
        def _():
            unit(slot)

    def z_msg(source, direction, hop):
        slot = (z + (NZ - hop + 1 if direction == 0 else hop - 1)) % NZ
        k = direction * 4 + hop - 1
        return remote(source, cz.at[slot], zss.at[k], zrs.at[k], zup if direction == 0 else zdn)

    def z_step(hop):
        for direction in (0, 1):
            if hop == 4 and direction == 1:
                continue
            slot = (z + (NZ - hop if direction == 0 else hop)) % NZ
            here = cz.at[slot]
            k = direction * 4 + hop - 1
            remote(here, here, zss.at[k], zrs.at[k], zup).wait_recv()
            if hop < 3 or (hop == 3 and direction == 0):
                go_send(z_msg(here, direction, hop + 1))

    for hop in range(2, 5):
        below, above = (z + NZ - hop + 1) % NZ, (z + hop - 1) % NZ
        poll(hop, first_half)
        against(below)
        if hop == 2:
            cx[x] = mine_x[...]
            for d in range(1, NX):
                x_msg(d, (x + NX - d) % NX).wait_recv()
            pa, pb = jnp.ones((1, 128), F32), jnp.zeros((1, 128), F32)
            ta, tb = pa, pb
            for i in range(NX):
                a, b = cx[i, 0:1, :], cx[i, 1:2, :]
                ta, tb = ta * a, a * tb + b
                pa = jnp.where(i < x, pa * a, pa)
                pb = jnp.where(i < x, a * pb + b, pb)
            mine_z[0:1, :] = ta
            mine_z[1:2, :] = tb
            for direction in (0, 1):
                go_send(z_msg(mine_z, direction, 1))
        else:
            z_step(hop - 2)
        poll(hop, second_half)
        against(above)
    against((z + 4) % NZ)

    def o_msg(d):
        return remote(po.at[d - 1], go.at[d - 1], oss.at[d - 1], ors.at[d - 1], xs[d])

    def s_msg(d):
        return remote(ps.at[d - 1], gs.at[d - 1], tss.at[d - 1], trs.at[d - 1], xs[d])

    for d in (2, 1, 3):
        xx = (x + d) % NX
        total = l_s[xx]
        ps[d - 1, 0:1, :] = m_s[xx]
        ps[d - 1, 1:2, :] = total
        po[d - 1] = (o_s[xx] / jnp.where(total > 0.0, total, 1.0)).astype(BF16)
        go_send(s_msg(d))
        go_send(o_msg(d))

    z_step(3)
    cz[z] = mine_z[...]
    z_step(4)
    entering = jnp.zeros((1, 128), F32)
    for i in range(NZ):
        entering = jnp.where(i < z, cz[i, 0:1, :] * entering + cz[i, 1:2, :], entering)
    entering = pa * entering + pb
    state = loc_s[...] + cum_s[...] * entering
    rec = state * jax.nn.gelu(gate_s[...])
    act_r[...] = (rec * rgain[...]).astype(BF16)
    square = (rec * rec).T
    sums[0:1, :] = jnp.sum(square, axis=0, keepdims=True)

    order = [(y + 2) % NY, (y + 1) % NY, (y + 3) % NY, y]
    mine = out_ref.shape[0]

    def rows_of(yy, cc):
        return pl.ds(pl.multiple_of((yy * 2 + cc) * mine, mine), mine)

    def r_msg(k):
        return remote(r_out.at[k], r_in.at[k], rss.at[k], rrs.at[k], {"tp": sib})

    def t_msg(k):
        return remote(t_out.at[k], t_in.at[k], pss.at[k], prs.at[k], {"tp": sib})

    for k, yy in enumerate(order):
        r_out[k] = mm(act_r[rows_of(yy, 1 - c), :], w_rec[...]).astype(BF16)
        go_send(r_msg(k))
    for k, yy in enumerate(order):
        r_own[k] = mm(act_r[rows_of(yy, c), :], w_rec[...])

    most = m_s[x]
    for d in range(1, NX):
        s_msg(d).wait_recv()
        most = jnp.maximum(most, gs[d - 1, 0:1, :])
    share = jnp.exp2(m_s[x] - most)
    total = l_s[x] * share
    out = o_s[x] * share
    for d in range(1, NX):
        o_msg(d).wait_recv()
        share = gs[d - 1, 1:2, :] * jnp.exp2(gs[d - 1, 0:1, :] - most)
        total = total + share
        out = out + go[d - 1].astype(F32) * share
    out = out / total
    sums[1:2, :] = jnp.sum(out * out, axis=0, keepdims=True)

    def sum_msg(d):
        return remote(sums, got_s.at[d - 1], sss.at[d - 1], srs.at[d - 1], {"tp": (tp + d) % NT})

    pl.semaphore_wait(hi.at[3], 1)
    for d in (4, 3, 5, 2, 6, 1, 7):
        go_send(sum_msg(d))
    act_t[...] = (out.T * again[...]).astype(BF16)
    for k, yy in enumerate(order):
        t_out[k] = mm(act_t[rows_of(yy, 1 - c), :], w_att[...]).astype(BF16)
        go_send(t_msg(k))
    for k, yy in enumerate(order):
        t_own[k] = mm(act_t[rows_of(yy, c), :], w_att[...])
    total = sums[...]
    for d in range(1, NT):
        sum_msg(d).wait_recv()
        total = total + got_s[d - 1]
    inverse = lax.rsqrt(total / (128 * NT) + EPS)
    inv_s[0] = jnp.broadcast_to(inverse[0:1, :], (128, rows)).T
    inv_s[1] = jnp.broadcast_to(inverse[1:2, :], (128, rows)).T

    def chip_sum(k):
        at = rows_of(order[k], c)
        r_msg(k).wait_recv()
        t_msg(k).wait_recv()
        value = (r_own[k] + r_in[k].astype(F32)) * inv_s[0, at, :][:, 0:1]
        return value + (t_own[k] + t_in[k].astype(F32)) * inv_s[1, at, :][:, 0:1]

    middle = model // 2
    left, right = pl.ds(0, middle), pl.ds(middle, middle)

    def f_msg(cols, k, to):
        return remote(f_out.at[:, cols], f_in.at[:, cols], fss.at[k], frs.at[k], {"tp": to})

    def n_msg(side, cols, k, to):
        at = (side, slice(None), cols)
        return remote(n_out.at[at], n_in_s.at[at], nss.at[k], nrs.at[k], {"tp": to})

    f_out[...] = chip_sum(0).astype(BF16)
    go_send(f_msg(left, 0, up))
    go_send(f_msg(right, 1, dn))
    part[0] = chip_sum(1)
    n_out[0, :, middle:] = part[0, :, middle:].astype(BF16)
    go_send(n_msg(0, right, 0, up))
    part[1] = chip_sum(2)
    n_out[1, :, 0:middle] = part[1, :, 0:middle].astype(BF16)
    go_send(n_msg(1, left, 1, dn))
    own = chip_sum(3)
    f_msg(left, 0, up).wait_recv()
    n_out[0, :, 0:middle] = (part[0, :, 0:middle] + f_in[:, 0:middle].astype(F32)).astype(BF16)
    go_send(n_msg(0, left, 2, up))
    f_msg(right, 1, dn).wait_recv()
    n_out[1, :, middle:] = (part[1, :, middle:] + f_in[:, middle:].astype(F32)).astype(BF16)
    go_send(n_msg(1, right, 3, dn))
    part[0] = own
    for k, (side, cols) in enumerate(((0, right), (1, left), (0, left), (1, right))):
        n_msg(side, cols, k, up).wait_recv()
    mixed = part[0] + n_in_s[0].astype(F32) + n_in_s[1].astype(F32)
    spread = lax.rsqrt(jnp.mean(mixed * mixed, axis=1, keepdims=True) + EPS)
    out_ref[...] = (mixed * spread * post[...]).astype(BF16)
    for copy in sent:
        copy.wait_send()


def call_layer(*operands):
    rows, depth = operands[0].shape
    model = depth * NT
    mine = rows // NT
    dma = pltpu.SemaphoreType.DMA
    vm = pltpu.VMEM
    scratch = [
        vm((NT, rows, depth), BF16), vm((1, model), F32), vm((model, 256), BF16),
        vm((QK + ROPE, model), BF16), vm((model, 512), BF16), vm((512, NOPE + VDIM), BF16),
        vm((1, 512), F32), vm((ROPE // 2, rows), F32), vm((ROPE // 2, rows), F32),
        vm((1, rows), F32), vm((4, 128), F32), vm((128, 128), BF16), vm((128, 128), BF16),
        vm((1, 128), F32), vm((1, 128), F32), vm((1, 128), F32), vm((128, model), BF16),
        vm((128, model), BF16), vm((1, model), F32),
        vm((rows, 256), F32), vm((rows, 256), F32), vm((rows, 512), F32), vm((rows, 128), F32),
        vm((QK + VDIM, rows), BF16), vm((QK, rows), BF16), vm((rows, 128), BF16),
        vm((rows, 128), F32), vm((NZ, QK + VDIM, rows), BF16), vm((NX, QK, rows), BF16),
        vm((16, 128), BF16), vm((16 + rows, 128), F32), vm((NX, 1, rows), F32),
        vm((NX, 1, rows), F32), vm((NX, VDIM, rows), F32), vm((rows, 128), F32),
        vm((rows, 128), F32),
        vm((2, 128), F32), vm((NX, 2, 128), F32), vm((2, 128), F32), vm((NZ, 2, 128), F32),
        vm((NX - 1, VDIM, rows), BF16), vm((NX - 1, 2, rows), F32),
        vm((NX - 1, VDIM, rows), BF16), vm((NX - 1, 2, rows), F32),
        vm((rows, 128), BF16), vm((rows, 128), BF16), vm((2, rows), F32),
        vm((NT - 1, 2, rows), F32), vm((2, rows, 128), F32),
        vm((NY, mine, model), BF16), vm((NY, mine, model), BF16), vm((NY, mine, model), F32),
        vm((NY, mine, model), BF16), vm((NY, mine, model), BF16), vm((NY, mine, model), F32),
        vm((2, mine, model), F32), vm((mine, model), BF16), vm((mine, model), BF16),
        vm((2, mine, model), BF16), vm((2, mine, model), BF16),
        dma((len(LOADS),)), pltpu.SemaphoreType.REGULAR((4,)),
        dma((13,)), dma((13,)), dma((8 * PIECES,)), dma((8 * PIECES,)),
        dma((NX - 1,)), dma((NX - 1,)), dma((2,)), dma((NX - 1,)), dma((NX - 1,)),
        dma((8,)), dma((8,)), dma((NX - 1,)), dma((NX - 1,)), dma((NX - 1,)), dma((NX - 1,)),
        dma((NT - 1,)), dma((NT - 1,)), dma((NY,)), dma((NY,)), dma((NY,)), dma((NY,)),
        dma((2,)), dma((2,)), dma((4,)), dma((4,)),
    ]
    return pl.pallas_call(
        layer,
        name="layer",
        out_shape=jax.ShapeDtypeStruct((mine, model), BF16),
        in_specs=[pl.BlockSpec(memory_space=pl.ANY)] * len(LOADS),
        out_specs=pl.BlockSpec(memory_space=pltpu.VMEM),
        scratch_shapes=scratch,
        compiler_params=pltpu.CompilerParams(
            collective_id=0, has_side_effects=True, vmem_limit_bytes=63 * 1024 * 1024
        ),
    )(*operands)


def shards(
    tokens, pre_gain, rate_factor, w_rec_in, w_rec_gate, conv_taps, rate_maps, input_maps,
    decay_param, w_query, w_latent, w_rope_key, latent_gain, w_expand, rec_gain, att_gain,
    w_out_rec, w_out_att, post_gain,
):
    rows = tokens.shape[0]
    frequency = 1.0 / THETA ** (jnp.arange(0, ROPE, 2).astype(F32) / ROPE)
    places = (lax.axis_index("sp") * rows + jnp.arange(rows)).astype(F32)
    turned = places[None, :] * frequency[:, None]
    given = {
        "tok": tokens, "gain": pre_gain[None], "w_in": w_rec_in, "w_gate": w_rec_gate,
        "w_q": w_query.T, "w_rope": w_rope_key.T, "w_lat": w_latent, "w_exp": w_expand,
        "lat_gain": latent_gain[None], "cos": jnp.cos(turned), "sin": jnp.sin(turned),
        "rf": rate_factor[None], "taps": conv_taps, "rmap": rate_maps[0], "imap": input_maps[0],
        "decay": decay_param[None], "rgain": rec_gain[None], "again": att_gain[None],
        "w_rec": w_out_rec, "w_att": w_out_att, "post": post_gain[None],
    }
    return call_layer(*(given[name] for name in LOADS))


def solution(mesh):
    placed = (
        P("sp", "tp"), P(), P("sp"), P(None, "tp"), P(None, "tp"), P(None, "tp"),
        P("tp", None, None), P("tp", None, None), P("tp"), P(None, "tp"), P(), P(), P(),
        P(None, "tp"), P("tp"), P("tp"), P("tp", None), P("tp", None), P(),
    )
    return jax.shard_map(
        shards, mesh=mesh, in_specs=placed, out_specs=P(("sp", "tp"), None), check_vma=False
    )
```

time: 220 us -> 67.9 us (0.31)
  the two profiles are of different devices: /device:TPU:228 before, /device:TPU:1 now
where the time goes in v2:
time: 67.9 us; the launch traced here: 67.8 us
  Pallas kernels  65.3 us (96%)
  local copies, waits for them, and re-layouts  1.67 us (2%)
  other arithmetic  0.84 us (1%)
    pallas_call x1, Pallas kernels, call_layer(): pl.pallas_call(layer, name='layer', out_shape=jax.ShapeDtypeStruct((mine,...  65.3 us
    unnamed x1, local copies, waits for them, and re-layouts  1.67 us

profile of v2, /device:TPU:1, one launch (start us, length us, event | category | flops | bytes accessed | tf_op | source)
XLA Modules:
  0.0 67.8 jit_solution(3857871439821859441)
XLA Ops:
  0.0 0.8 %multiply_sine_fusion = (f32[32,256]{1,0:T(8,128)}, f32[32,256]{1,0:T(8,128)}) fusion(f32[32]{0:T(128)S(1)} %negate_power_fusion, f32[256]{0:T(256)S(1)} %add_convert_fusion), kind=kLoop, calls=%fused_computation | loop fusion | flops 8192 | bytes 66688 | tf_op jit(solution)/shard_map/sin | solution.py:577
  0.8 65.3 %layer.1 = bf16[32,4096]{1,0:T(8,128)(2,1)} custom-call(bf16[256,512]{1,0:T(8,128)(2,1)} %refs_0_.1, f32[1,4096]{1,0:T(1,128)} %bitcast.15, bf16[4096,128]{1,0:T(8,128)(2,1)} %refs_2_.1, bf16[4096,128]{1,0:T(8,128)(2,1)} %refs_3_.1, bf16[192,4096]{1,0:T(8,128)(2,1)} %bitcast.11, bf16[64,4096]{1,0:T(8,128)(2,1)} %bitcast.12, bf16[4096,512]{1,0:T(8,128)(2,1)} %refs_6_.1, ...), custom_call_target="tpu_custom_call" | custom-call | tf_op jit(solution)/shard_map/layer/pallas_call | solution.py:552
  66.1 1.7 %copy.21 = bf16[32,4096]{1,0:T(8,128)(2,1)} copy(bf16[32,4096]{1,0:T(8,128)(2,1)} %layer.1) | data formatting | bytes 524288
  (2 shorter events, 0.0 us)

commit v3 on v2

--- a/solution.py
+++ b/solution.py
@@ -85,11 +85,12 @@
         a_ig, a_qr, a_lat, sq,
         own_kv, own_q, rec_s, gate_s, kv, qs, halo, ext, m_s, l_s, o_s, cum_s, loc_s,
         mine_x, cx, mine_z, cz, po, ps, go, gs,
-        act_r, act_t, sums, got_s, inv_s, r_out, r_in, r_own, t_out, t_in, t_own,
-        part, f_out, f_in, n_out, n_in_s,
+        act_r, act_t, sums, got_s, inv_s, part,
         lsem, hi, ass, ars, kss, krs, qss, qrs, hsem, xss, xrs, zss, zrs, oss, ors, tss, trs,
-        sss, srs, rss, rrs, pss, prs, fss, frs, nss, nrs,
+        sss, srs, *rest,
     ) = refs[n_in + 1 :]
+    r_bufs, t_bufs = rest[0:7], rest[7:14]
+    r_sems, t_sems = rest[14:20], rest[20:26]
 
     sp, tp = lax.axis_index("sp"), lax.axis_index("tp")
     z, x = sp // NX, sp % NX
@@ -123,12 +124,13 @@
         name: pltpu.make_async_copy(src[name], where[name], lsem.at[k])
         for k, name in enumerate(LOADS)
     }
-    for name in LOADS:
-        load[name].start()
+    load["tok"].start()
     greet([{"tp": sib}, {"tp": up}, {"tp": dn}, xs[1], xs[3], zup, zdn])
     hello(hi.at[0], xs[3])
     hello(hi.at[1], {"tp": dn})
     hello(hi.at[2], {"tp": sib})
+    hello(hi.at[4], zdn)
+    hello(hi.at[5], zup)
 
     sent = []
 
@@ -154,6 +156,8 @@
     send(0, tp, whole, sib)
     send(2, tp, h1, up)
     send(4, tp, h0, dn)
+    for name in LOADS[1:]:
+        load[name].start()
 
     def chunk(source, first=False):
         wide = tok[source].astype(F32)
@@ -177,6 +181,10 @@
     chunk(tp, True)
     pl.semaphore_wait(hi.at[2], 1)
     hello(hi.at[3], {"tp": dn})
+    pl.semaphore_wait(hi.at[4], 1)
+    hello(hi.at[6], zdn)
+    pl.semaphore_wait(hi.at[5], 1)
+    hello(hi.at[7], zup)
     arrived(0, sib, whole)
     chunk(sib)
     arrived(1, dn, h0)
@@ -190,6 +198,9 @@
     arrived(4, up, h0)
     send(10, up, h0, sib)
     chunk(dn)
+    pl.semaphore_wait(hi.at[6], 1)
+    hello(hi.at[8], zdn)
+    pl.semaphore_wait(hi.at[7], 1)
     chunk(up)
     arrived(7, dn_sib, h0)
     arrived(8, dn_sib, h1)
@@ -209,6 +220,12 @@
     chunk(far_sib)
 
     inverse = lax.rsqrt(jnp.sum(sq[...], axis=1, keepdims=True) / model + EPS)
+    rec_s[...] = (inverse * a_ig[:, 0:128]).astype(BF16)
+    succ = {"sp": (sp + 1) % (NX * NZ)}
+    tail = rows - 16
+    pl.semaphore_wait(hi.at[0], 1)
+    mine_tail = remote(rec_s.at[pl.ds(tail, 16)], halo, hsem.at[0], hsem.at[1], succ)
+    go_send(mine_tail)
     latent = inverse * a_lat[...]
     spread = lax.rsqrt(jnp.mean(latent * latent, axis=1, keepdims=True) + EPS)
     latent = (latent * spread * lat_gain[...]).astype(BF16)
@@ -245,19 +262,15 @@
     own_q[0:NOPE, :] = (inverse * a_qr[:, 0:NOPE]).T.astype(BF16)
     own_q[NOPE : NOPE + hr, :] = (u * cosine - w * sine).astype(BF16)
     own_q[NOPE + hr :, :] = (w * cosine + u * sine).astype(BF16)
-    rec_s[...] = (inverse * a_ig[:, 0:128]).astype(BF16)
-    gate_s[...] = inverse * a_ig[:, 128:256]
-    succ = {"sp": (sp + 1) % (NX * NZ)}
-    tail = rows - 16
-
-    pl.semaphore_wait(hi.at[0], 1)
-    pl.semaphore_wait(hi.at[1], 1)
 
     def q_msg(d, slot):
         return remote(own_q, qs.at[slot], qss.at[d - 1], qrs.at[d - 1], xs[d])
 
-    for d in (2, 1, 3):
-        go_send(q_msg(d, x))
+    go_send(q_msg(1, x))
+    go_send(q_msg(3, x))
+    gate_s[...] = inverse * a_ig[:, 128:256]
+    pl.semaphore_wait(hi.at[1], 1)
+    pl.semaphore_wait(hi.at[8], 1)
 
     for xx in range(NX):
         m_s[xx] = jnp.full((1, rows), LOW, F32)
@@ -300,12 +313,98 @@
 
     first_half, second_half = (0, 1), (2, 3)
 
+    def against(slot):
+        @pl.when(slot < z)
+        def _():
+            unit(slot)
+
+    def below(hop):
+        against((z + NZ - hop) % NZ)
+
+    def above(hop):
+        against((z + hop) % NZ)
+
+    order = [(y + 2) % NY, (y + 1) % NY, (y + 3) % NY, y]
+    mine = out_ref.shape[0]
+    middle = model // 2
+    left, right = pl.ds(0, middle), pl.ds(middle, middle)
+
+    def rows_of(yy, cc):
+        return pl.ds(pl.multiple_of((yy * 2 + cc) * mine, mine), mine)
+
+    class Branch:
+        def __init__(self, act, weight, bufs, sems):
+            self.act, self.weight = act, weight
+            self.out, self.got, self.own, self.f_out, self.f_in, self.n_out, self.n_in = bufs
+            self.ps, self.pr, self.fs, self.fr, self.ns, self.nr = sems
+
+        def pair(self, k):
+            return remote(self.out.at[k], self.got.at[k], self.ps.at[k], self.pr.at[k], {"tp": sib})
+
+        def far(self, k):
+            cols, to = ((left, up), (right, dn))[k]
+            return remote(
+                self.f_out.at[:, cols], self.f_in.at[:, cols], self.fs.at[k], self.fr.at[k], {"tp": to}
+            )
+
+        def near(self, k):
+            side, cols = ((0, right), (1, left), (0, left), (1, right))[k]
+            at = (side, slice(None), cols)
+            return remote(
+                self.n_out.at[at], self.n_in.at[at], self.ns.at[k], self.nr.at[k],
+                {"tp": (up, dn)[side]},
+            )
+
+        def product(self, k):
+            yy = order[k]
+            both = jnp.concatenate(
+                [self.act[rows_of(yy, 1 - c), :], self.act[rows_of(yy, c), :]], axis=0
+            )
+            value = mm(both, self.weight[...])
+            self.out[k] = value[0:mine].astype(BF16)
+            go_send(self.pair(k))
+            self.own[k] = value[mine:]
+
+        def chip(self, k):
+            self.pair(k).wait_recv()
+            return self.own[k] + self.got[k].astype(F32)
+
+        def send_far(self):
+            self.f_out[...] = self.chip(0).astype(BF16)
+            go_send(self.far(0))
+            go_send(self.far(1))
+
+        def send_pure(self):
+            up_sum = self.chip(1)
+            self.n_out[0, :, middle:] = up_sum[:, middle:].astype(BF16)
+            go_send(self.near(0))
+            self.own[1, :, 0:middle] = up_sum[:, 0:middle]
+            dn_sum = self.chip(2)
+            self.n_out[1, :, 0:middle] = dn_sum[:, 0:middle].astype(BF16)
+            go_send(self.near(1))
+            self.own[2, :, middle:] = dn_sum[:, middle:]
+            self.own[3] = self.chip(3)
+
+        def send_joined(self):
+            self.far(0).wait_recv()
+            joined = self.own[1, :, 0:middle] + self.f_in[:, 0:middle].astype(F32)
+            self.n_out[0, :, 0:middle] = joined.astype(BF16)
+            go_send(self.near(2))
+            self.far(1).wait_recv()
+            joined = self.own[2, :, middle:] + self.f_in[:, middle:].astype(F32)
+            self.n_out[1, :, middle:] = joined.astype(BF16)
+            go_send(self.near(3))
+
+        def total(self):
+            for k in range(4):
+                self.near(k).wait_recv()
+            return self.own[3] + self.n_in[0].astype(F32) + self.n_in[1].astype(F32)
+
+    branch_r = Branch(act_r, w_rec, r_bufs, r_sems)
+    branch_t = Branch(act_t, w_att, t_bufs, t_sems)
+
     ext[16:, :] = rec_s[...].astype(F32)
-    mine_tail = remote(rec_s.at[pl.ds(tail, 16)], halo, hsem.at[0], hsem.at[1], succ)
-    go_send(mine_tail)
-    own_k = own_kv[0:QK, :].T
-    attend((x,), [own_q[...]], own_k, own_kv[QK:, :], True)
-    poll(1, first_half)
+    attend((x,), [own_q[...]], own_kv[0:QK, :].T, own_kv[QK:, :], True)
     mine_tail.wait_recv()
     ext[0:16, :] = jnp.where(sp == 0, 0.0, halo[...].astype(F32))
     convolved = taps[0:1, :] * ext[13 : 13 + rows, :]
@@ -331,12 +430,35 @@
     def x_msg(d, slot):
         return remote(mine_x, cx.at[slot], xss.at[d - 1], xrs.at[d - 1], xs[d])
 
+    for d in (2, 1, 3):
+        go_send(x_msg(d, x))
+    go_send(q_msg(2, x))
+    poll(1, first_half)
+    poll(1, second_half)
+
+    cx[x] = mine_x[...]
     for d in range(1, NX):
-        go_send(x_msg(d, x))
-    poll(1, second_half)
-
+        x_msg(d, (x + NX - d) % NX).wait_recv()
+    pa, pb = jnp.ones((1, 128), F32), jnp.zeros((1, 128), F32)
+    ta, tb = pa, pb
+    for i in range(NX):
+        a, b = cx[i, 0:1, :], cx[i, 1:2, :]
+        ta, tb = ta * a, a * tb + b
+        pa = jnp.where(i < x, pa * a, pa)
+        pb = jnp.where(i < x, a * pb + b, pb)
+    mine_z[0:1, :] = ta
+    mine_z[1:2, :] = tb
+
+    def z_msg(d, slot):
+        to = at_zx((z + d) % NZ, x)
+        return remote(mine_z, cz.at[slot], zss.at[d - 1], zrs.at[d - 1], to)
+
+    for d in (4, 3, 5, 2, 6, 1, 7):
+        go_send(z_msg(d, z))
+
+    poll(2, first_half)
     qs[x] = own_q[...]
-    for d in range(1, NX):
+    for d in (1, 3, 2):
         q_msg(d, (x + NX - d) % NX).wait_recv()
     for xx in range(1, NX):
 
@@ -344,70 +466,14 @@
         def _():
             attend((xx,), [qs[xx]], own_kv[0:QK, :].T, own_kv[QK:, :], False)
 
-    def against(slot):
-        @pl.when(slot < z)
-        def _():
-            unit(slot)
-
-    def z_msg(source, direction, hop):
-        slot = (z + (NZ - hop + 1 if direction == 0 else hop - 1)) % NZ
-        k = direction * 4 + hop - 1
-        return remote(source, cz.at[slot], zss.at[k], zrs.at[k], zup if direction == 0 else zdn)
-
-    def z_step(hop):
-        for direction in (0, 1):
-            if hop == 4 and direction == 1:
-                continue
-            slot = (z + (NZ - hop if direction == 0 else hop)) % NZ
-            here = cz.at[slot]
-            k = direction * 4 + hop - 1
-            remote(here, here, zss.at[k], zrs.at[k], zup).wait_recv()
-            if hop < 3 or (hop == 3 and direction == 0):
-                go_send(z_msg(here, direction, hop + 1))
-
-    for hop in range(2, 5):
-        below, above = (z + NZ - hop + 1) % NZ, (z + hop - 1) % NZ
-        poll(hop, first_half)
-        against(below)
-        if hop == 2:
-            cx[x] = mine_x[...]
-            for d in range(1, NX):
-                x_msg(d, (x + NX - d) % NX).wait_recv()
-            pa, pb = jnp.ones((1, 128), F32), jnp.zeros((1, 128), F32)
-            ta, tb = pa, pb
-            for i in range(NX):
-                a, b = cx[i, 0:1, :], cx[i, 1:2, :]
-                ta, tb = ta * a, a * tb + b
-                pa = jnp.where(i < x, pa * a, pa)
-                pb = jnp.where(i < x, a * pb + b, pb)
-            mine_z[0:1, :] = ta
-            mine_z[1:2, :] = tb
-            for direction in (0, 1):
-                go_send(z_msg(mine_z, direction, 1))
-        else:
-            z_step(hop - 2)
-        poll(hop, second_half)
-        against(above)
-    against((z + 4) % NZ)
-
-    def o_msg(d):
-        return remote(po.at[d - 1], go.at[d - 1], oss.at[d - 1], ors.at[d - 1], xs[d])
-
-    def s_msg(d):
-        return remote(ps.at[d - 1], gs.at[d - 1], tss.at[d - 1], trs.at[d - 1], xs[d])
-
-    for d in (2, 1, 3):
-        xx = (x + d) % NX
-        total = l_s[xx]
-        ps[d - 1, 0:1, :] = m_s[xx]
-        ps[d - 1, 1:2, :] = total
-        po[d - 1] = (o_s[xx] / jnp.where(total > 0.0, total, 1.0)).astype(BF16)
-        go_send(s_msg(d))
-        go_send(o_msg(d))
-
-    z_step(3)
+    poll(2, second_half)
+    below(1)
+    poll(3, first_half)
+    above(1)
+
     cz[z] = mine_z[...]
-    z_step(4)
+    for d in range(1, NZ):
+        z_msg(d, (z + NZ - d) % NZ).wait_recv()
     entering = jnp.zeros((1, 128), F32)
     for i in range(NZ):
         entering = jnp.where(i < z, cz[i, 0:1, :] * entering + cz[i, 1:2, :], entering)
@@ -417,24 +483,37 @@
     act_r[...] = (rec * rgain[...]).astype(BF16)
     square = (rec * rec).T
     sums[0:1, :] = jnp.sum(square, axis=0, keepdims=True)
-
-    order = [(y + 2) % NY, (y + 1) % NY, (y + 3) % NY, y]
-    mine = out_ref.shape[0]
-
-    def rows_of(yy, cc):
-        return pl.ds(pl.multiple_of((yy * 2 + cc) * mine, mine), mine)
-
-    def r_msg(k):
-        return remote(r_out.at[k], r_in.at[k], rss.at[k], rrs.at[k], {"tp": sib})
-
-    def t_msg(k):
-        return remote(t_out.at[k], t_in.at[k], pss.at[k], prs.at[k], {"tp": sib})
-
-    for k, yy in enumerate(order):
-        r_out[k] = mm(act_r[rows_of(yy, 1 - c), :], w_rec[...]).astype(BF16)
-        go_send(r_msg(k))
-    for k, yy in enumerate(order):
-        r_own[k] = mm(act_r[rows_of(yy, c), :], w_rec[...])
+    for k in (0, 1):
+        branch_r.product(k)
+    poll(3, second_half)
+    for k in (2, 3):
+        branch_r.product(k)
+    branch_r.send_far()
+    below(2)
+    poll(4, first_half)
+    branch_r.send_pure()
+    above(2)
+    below(3)
+    poll(4, second_half)
+    above(3)
+    below(4)
+
+    def o_msg(d):
+        return remote(po.at[d - 1], go.at[d - 1], oss.at[d - 1], ors.at[d - 1], xs[d])
+
+    def s_msg(d):
+        return remote(ps.at[d - 1], gs.at[d - 1], tss.at[d - 1], trs.at[d - 1], xs[d])
+
+    for d in (2, 1, 3):
+        xx = (x + d) % NX
+        total = l_s[xx]
+        ps[d - 1, 0:1, :] = m_s[xx]
+        ps[d - 1, 1:2, :] = total
+        po[d - 1] = (o_s[xx] / jnp.where(total > 0.0, total, 1.0)).astype(BF16)
+        go_send(s_msg(d))
+        go_send(o_msg(d))
+
+    branch_r.send_joined()
 
     most = m_s[x]
     for d in range(1, NX):
@@ -458,11 +537,12 @@
     for d in (4, 3, 5, 2, 6, 1, 7):
         go_send(sum_msg(d))
     act_t[...] = (out.T * again[...]).astype(BF16)
-    for k, yy in enumerate(order):
-        t_out[k] = mm(act_t[rows_of(yy, 1 - c), :], w_att[...]).astype(BF16)
-        go_send(t_msg(k))
-    for k, yy in enumerate(order):
-        t_own[k] = mm(act_t[rows_of(yy, c), :], w_att[...])
+    branch_t.product(0)
+    branch_t.product(1)
+    branch_t.send_far()
+    branch_t.product(2)
+    branch_t.product(3)
+    branch_t.send_pure()
     total = sums[...]
     for d in range(1, NT):
         sum_msg(d).wait_recv()
@@ -470,44 +550,10 @@
     inverse = lax.rsqrt(total / (128 * NT) + EPS)
     inv_s[0] = jnp.broadcast_to(inverse[0:1, :], (128, rows)).T
     inv_s[1] = jnp.broadcast_to(inverse[1:2, :], (128, rows)).T
-
-    def chip_sum(k):
-        at = rows_of(order[k], c)
-        r_msg(k).wait_recv()
-        t_msg(k).wait_recv()
-        value = (r_own[k] + r_in[k].astype(F32)) * inv_s[0, at, :][:, 0:1]
-        return value + (t_own[k] + t_in[k].astype(F32)) * inv_s[1, at, :][:, 0:1]
-
-    middle = model // 2
-    left, right = pl.ds(0, middle), pl.ds(middle, middle)
-
-    def f_msg(cols, k, to):
-        return remote(f_out.at[:, cols], f_in.at[:, cols], fss.at[k], frs.at[k], {"tp": to})
-
-    def n_msg(side, cols, k, to):
-        at = (side, slice(None), cols)
-        return remote(n_out.at[at], n_in_s.at[at], nss.at[k], nrs.at[k], {"tp": to})
-
-    f_out[...] = chip_sum(0).astype(BF16)
-    go_send(f_msg(left, 0, up))
-    go_send(f_msg(right, 1, dn))
-    part[0] = chip_sum(1)
-    n_out[0, :, middle:] = part[0, :, middle:].astype(BF16)
-    go_send(n_msg(0, right, 0, up))
-    part[1] = chip_sum(2)
-    n_out[1, :, 0:middle] = part[1, :, 0:middle].astype(BF16)
-    go_send(n_msg(1, left, 1, dn))
-    own = chip_sum(3)
-    f_msg(left, 0, up).wait_recv()
-    n_out[0, :, 0:middle] = (part[0, :, 0:middle] + f_in[:, 0:middle].astype(F32)).astype(BF16)
-    go_send(n_msg(0, left, 2, up))
-    f_msg(right, 1, dn).wait_recv()
-    n_out[1, :, middle:] = (part[1, :, middle:] + f_in[:, middle:].astype(F32)).astype(BF16)
-    go_send(n_msg(1, right, 3, dn))
-    part[0] = own
-    for k, (side, cols) in enumerate(((0, right), (1, left), (0, left), (1, right))):
-        n_msg(side, cols, k, up).wait_recv()
-    mixed = part[0] + n_in_s[0].astype(F32) + n_in_s[1].astype(F32)
+    at = rows_of(y, c)
+    part[0] = branch_r.total() * inv_s[0, at, :][:, 0:1]
+    branch_t.send_joined()
+    mixed = part[0] + branch_t.total() * inv_s[1, at, :][:, 0:1]
     spread = lax.rsqrt(jnp.mean(mixed * mixed, axis=1, keepdims=True) + EPS)
     out_ref[...] = (mixed * spread * post[...]).astype(BF16)
     for copy in sent:
@@ -538,17 +584,21 @@
         vm((NX - 1, VDIM, rows), BF16), vm((NX - 1, 2, rows), F32),
         vm((rows, 128), BF16), vm((rows, 128), BF16), vm((2, rows), F32),
         vm((NT - 1, 2, rows), F32), vm((2, rows, 128), F32),
-        vm((NY, mine, model), BF16), vm((NY, mine, model), BF16), vm((NY, mine, model), F32),
-        vm((NY, mine, model), BF16), vm((NY, mine, model), BF16), vm((NY, mine, model), F32),
-        vm((2, mine, model), F32), vm((mine, model), BF16), vm((mine, model), BF16),
-        vm((2, mine, model), BF16), vm((2, mine, model), BF16),
-        dma((len(LOADS),)), pltpu.SemaphoreType.REGULAR((4,)),
+        vm((1, mine, model), F32),
+        dma((len(LOADS),)), pltpu.SemaphoreType.REGULAR((9,)),
         dma((13,)), dma((13,)), dma((8 * PIECES,)), dma((8 * PIECES,)),
         dma((NX - 1,)), dma((NX - 1,)), dma((2,)), dma((NX - 1,)), dma((NX - 1,)),
         dma((8,)), dma((8,)), dma((NX - 1,)), dma((NX - 1,)), dma((NX - 1,)), dma((NX - 1,)),
-        dma((NT - 1,)), dma((NT - 1,)), dma((NY,)), dma((NY,)), dma((NY,)), dma((NY,)),
-        dma((2,)), dma((2,)), dma((4,)), dma((4,)),
+        dma((NT - 1,)), dma((NT - 1,)),
     ]
+    for _ in range(2):
+        scratch += [
+            vm((NY, mine, model), BF16), vm((NY, mine, model), BF16), vm((NY, mine, model), F32),
+            vm((mine, model), BF16), vm((mine, model), BF16),
+            vm((2, mine, model), BF16), vm((2, mine, model), BF16),
+        ]
+    for _ in range(2):
+        scratch += [dma((NY,)), dma((NY,)), dma((2,)), dma((2,)), dma((4,)), dma((4,))]
     return pl.pallas_call(
         layer,
         name="layer",

time: 67.9 us -> 62.1 us (0.915)
  Pallas kernels: 65.3 us -> 59.4 us
    pallas_call x1, Pallas kernels: 65.3 us -> 59.4 us  [call_layer(): pl.pallas_call(layer, name='layer', out_shape=jax.ShapeDtypeStruct((mine,...]
where the time goes in v3:
time: 62.1 us; the launch traced here: 61.9 us
  Pallas kernels  59.4 us (96%)
  local copies, waits for them, and re-layouts  1.67 us (3%)
  other arithmetic  0.84 us (1%)
    pallas_call x1, Pallas kernels, call_layer(): pl.pallas_call(layer, name='layer', out_shape=jax.ShapeDtypeStruct((mine,...  59.4 us
    unnamed x1, local copies, waits for them, and re-layouts  1.67 us

profile of v3, /device:TPU:1, one launch (start us, length us, event | category | flops | bytes accessed | tf_op | source)
XLA Modules:
  0.0 61.9 jit_solution(15891763176870800948)
XLA Ops:
  0.0 0.8 %multiply_sine_fusion = (f32[32,256]{1,0:T(8,128)}, f32[32,256]{1,0:T(8,128)}) fusion(f32[32]{0:T(128)S(1)} %negate_power_fusion, f32[256]{0:T(256)S(1)} %add_convert_fusion), kind=kLoop, calls=%fused_computation | loop fusion | flops 8192 | bytes 66688 | tf_op jit(solution)/shard_map/sin | solution.py:627
  0.8 59.4 %layer.1 = bf16[32,4096]{1,0:T(8,128)(2,1)} custom-call(bf16[256,512]{1,0:T(8,128)(2,1)} %refs_0_.1, f32[1,4096]{1,0:T(1,128)} %bitcast.15, bf16[4096,128]{1,0:T(8,128)(2,1)} %refs_2_.1, bf16[4096,128]{1,0:T(8,128)(2,1)} %refs_3_.1, bf16[192,4096]{1,0:T(8,128)(2,1)} %bitcast.11, bf16[64,4096]{1,0:T(8,128)(2,1)} %bitcast.12, bf16[4096,512]{1,0:T(8,128)(2,1)} %refs_6_.1, ...), custom_call_target="tpu_custom_call" | custom-call | tf_op jit(solution)/shard_map/layer/pallas_call | solution.py:602
  60.3 1.7 %copy.21 = bf16[32,4096]{1,0:T(8,128)(2,1)} copy(bf16[32,4096]{1,0:T(8,128)(2,1)} %layer.1) | data formatting | bytes 524288
  (2 shorter events, 0.0 us)

commit v4 on v3

--- a/solution.py
+++ b/solution.py
@@ -2,6 +2,7 @@
 
 import jax
 import jax.numpy as jnp
+import numpy as np
 from jax import lax
 from jax.experimental import pallas as pl
 from jax.experimental.pallas import tpu as pltpu
@@ -70,7 +71,7 @@
 
 
 LOADS = (
-    "tok", "gain", "w_in", "w_gate", "w_q", "w_rope", "w_lat", "w_exp", "lat_gain", "cos", "sin",
+    "tok", "gain", "w_in", "w_gate", "w_q", "w_rope", "w_lat", "w_exp", "lat_gain", "freq",
     "rf", "taps", "rmap", "imap", "decay", "rgain", "again", "w_rec", "w_att", "post",
 )
 
@@ -80,17 +81,17 @@
     src = dict(zip(LOADS, refs[:n_in]))
     out_ref = refs[n_in]
     (
-        tok, gain, v_ig, v_qr, v_lat, v_exp, lat_gain, cos_s, sin_s, rf, taps, rmap, imap, decay,
+        tok, gain, v_ig, v_qr, v_lat, v_exp, lat_gain, freq, cos_s, sin_s, rf, taps, rmap, imap, decay,
         rgain, again, w_rec, w_att, post,
         a_ig, a_qr, a_lat, sq,
         own_kv, own_q, rec_s, gate_s, kv, qs, halo, ext, m_s, l_s, o_s, cum_s, loc_s,
         mine_x, cx, mine_z, cz, po, ps, go, gs,
-        act_r, act_t, sums, got_s, inv_s, part,
+        sums, got_s, inv_s, part,
         lsem, hi, ass, ars, kss, krs, qss, qrs, hsem, xss, xrs, zss, zrs, oss, ors, tss, trs,
-        sss, srs, *rest,
+        sss, srs, wss, wrs, *rest,
     ) = refs[n_in + 1 :]
-    r_bufs, t_bufs = rest[0:7], rest[7:14]
-    r_sems, t_sems = rest[14:20], rest[20:26]
+    r_bufs, t_bufs = rest[0:8], rest[8:16]
+    r_sems, t_sems = rest[16:22], rest[22:28]
 
     sp, tp = lax.axis_index("sp"), lax.axis_index("tp")
     z, x = sp // NX, sp % NX
@@ -113,12 +114,13 @@
     model = depth * NT
     half = rows // 2
 
+    mine_rows = pl.ds(pl.multiple_of(c * 128, 128), 128)
     where = {
         "tok": tok.at[tp], "gain": gain, "w_in": v_ig.at[:, pl.ds(0, 128)],
         "w_gate": v_ig.at[:, pl.ds(128, 128)], "w_q": v_qr.at[pl.ds(0, QK)],
         "w_rope": v_qr.at[pl.ds(QK, ROPE)], "w_lat": v_lat, "w_exp": v_exp, "lat_gain": lat_gain,
-        "cos": cos_s, "sin": sin_s, "rf": rf, "taps": taps, "rmap": rmap, "imap": imap,
-        "decay": decay, "rgain": rgain, "again": again, "w_rec": w_rec, "w_att": w_att, "post": post,
+        "freq": freq, "rf": rf, "taps": taps, "rmap": rmap, "imap": imap,
+        "decay": decay, "rgain": rgain, "again": again, "w_rec": w_rec.at[mine_rows], "w_att": w_att.at[mine_rows], "post": post,
     }
     load = {
         name: pltpu.make_async_copy(src[name], where[name], lsem.at[k])
@@ -187,6 +189,12 @@
     hello(hi.at[7], zup)
     arrived(0, sib, whole)
     chunk(sib)
+    for name in LOADS[7:]:
+        load[name].wait()
+    places = lax.broadcasted_iota(jnp.int32, (ROPE // 2, rows), 1) + sp * rows
+    angle = places.astype(F32) * freq[...]
+    cos_s[...] = jnp.cos(angle)
+    sin_s[...] = jnp.sin(angle)
     arrived(1, dn, h0)
     send(5, dn, h0, up)
     send(7, dn, h0, sib)
@@ -213,8 +221,6 @@
     arrived(6, far, h1)
     send(12, far, h1, sib)
     chunk(far)
-    for name in LOADS[7:]:
-        load[name].wait()
     arrived(11, far_sib, h0)
     arrived(12, far_sib, h1)
     chunk(far_sib)
@@ -254,9 +260,20 @@
     def kv_goes(direction, hop, p):
         return hop < 4 or (hop == 4 and (direction == 0) == (p < PIECES // 2))
 
-    for p in range(PIECES):
+    def piece(direction, i):
+        return (i + 2 * direction) % PIECES
+
+    for i in range(PIECES):
         for direction in (0, 1):
+            p = piece(direction, i)
             go_send(kv_msg(own_kv.at[piece_at(p)], direction, 1, p))
+
+    def w_msg(weight, k):
+        at = weight.at[mine_rows]
+        return remote(at, at, wss.at[k], wrs.at[k], {"tp": sib})
+
+    go_send(w_msg(w_rec, 0))
+    go_send(w_msg(w_att, 1))
 
     u, w = turned[0:hr], turned[hr:ROPE]
     own_q[0:NOPE, :] = (inverse * a_qr[:, 0:NOPE]).T.astype(BF16)
@@ -301,8 +318,9 @@
         )
 
     def poll(hop, pieces):
-        for p in pieces:
+        for i in pieces:
             for direction in (0, 1):
+                p = piece(direction, i)
                 if kv_goes(direction, hop, p):
                     slot = (z + (NZ - hop if direction == 0 else hop)) % NZ
                     here = kv.at[slot, piece_at(p)]
@@ -333,13 +351,14 @@
         return pl.ds(pl.multiple_of((yy * 2 + cc) * mine, mine), mine)
 
     class Branch:
-        def __init__(self, act, weight, bufs, sems):
-            self.act, self.weight = act, weight
-            self.out, self.got, self.own, self.f_out, self.f_in, self.n_out, self.n_in = bufs
+        def __init__(self, weight, k, bufs, sems):
+            self.weight, self.k = weight, k
+            self.natural, self.out, self.act, self.own, self.f_out, self.f_in, self.n_out, self.n_in = bufs
             self.ps, self.pr, self.fs, self.fr, self.ns, self.nr = sems
 
-        def pair(self, k):
-            return remote(self.out.at[k], self.got.at[k], self.ps.at[k], self.pr.at[k], {"tp": sib})
+        def pair(self):
+            at = self.act.at[:, mine_rows]
+            return remote(self.out, at, self.ps.at[0], self.pr.at[0], {"tp": sib})
 
         def far(self, k):
             cols, to = ((left, up), (right, dn))[k]
@@ -355,53 +374,45 @@
                 {"tp": (up, dn)[side]},
             )
 
-        def product(self, k):
-            yy = order[k]
-            both = jnp.concatenate(
-                [self.act[rows_of(yy, 1 - c), :], self.act[rows_of(yy, c), :]], axis=0
-            )
-            value = mm(both, self.weight[...])
-            self.out[k] = value[0:mine].astype(BF16)
-            go_send(self.pair(k))
-            self.own[k] = value[mine:]
-
-        def chip(self, k):
-            self.pair(k).wait_recv()
-            return self.own[k] + self.got[k].astype(F32)
+        def begin(self, value):
+            self.natural[...] = value
+            for k, yy in enumerate(order):
+                at = slice(k * mine, (k + 1) * mine)
+                self.out[at, :] = self.natural[rows_of(yy, 1 - c), :]
+                self.act[at, mine_rows] = self.natural[rows_of(yy, c), :]
+            go_send(self.pair())
 
         def send_far(self):
-            self.f_out[...] = self.chip(0).astype(BF16)
+            w_msg(self.weight, self.k).wait_recv()
+            self.pair().wait_recv()
+            self.f_out[...] = mm(self.act[0:mine, :], self.weight[...]).astype(BF16)
             go_send(self.far(0))
             go_send(self.far(1))
 
         def send_pure(self):
-            up_sum = self.chip(1)
-            self.n_out[0, :, middle:] = up_sum[:, middle:].astype(BF16)
+            self.own[...] = mm(self.act[mine:, :], self.weight[...])
+            self.n_out[0, :, middle:] = self.own[0:mine, middle:].astype(BF16)
             go_send(self.near(0))
-            self.own[1, :, 0:middle] = up_sum[:, 0:middle]
-            dn_sum = self.chip(2)
-            self.n_out[1, :, 0:middle] = dn_sum[:, 0:middle].astype(BF16)
+            self.n_out[1, :, 0:middle] = self.own[mine : 2 * mine, 0:middle].astype(BF16)
             go_send(self.near(1))
-            self.own[2, :, middle:] = dn_sum[:, middle:]
-            self.own[3] = self.chip(3)
 
         def send_joined(self):
             self.far(0).wait_recv()
-            joined = self.own[1, :, 0:middle] + self.f_in[:, 0:middle].astype(F32)
+            joined = self.own[0:mine, 0:middle] + self.f_in[:, 0:middle].astype(F32)
             self.n_out[0, :, 0:middle] = joined.astype(BF16)
             go_send(self.near(2))
             self.far(1).wait_recv()
-            joined = self.own[2, :, middle:] + self.f_in[:, middle:].astype(F32)
+            joined = self.own[mine : 2 * mine, middle:] + self.f_in[:, middle:].astype(F32)
             self.n_out[1, :, middle:] = joined.astype(BF16)
             go_send(self.near(3))
 
         def total(self):
             for k in range(4):
                 self.near(k).wait_recv()
-            return self.own[3] + self.n_in[0].astype(F32) + self.n_in[1].astype(F32)
-
-    branch_r = Branch(act_r, w_rec, r_bufs, r_sems)
-    branch_t = Branch(act_t, w_att, t_bufs, t_sems)
+            return self.own[2 * mine :, :] + self.n_in[0].astype(F32) + self.n_in[1].astype(F32)
+
+    branch_r = Branch(w_rec, 0, r_bufs, r_sems)
+    branch_t = Branch(w_att, 1, t_bufs, t_sems)
 
     ext[16:, :] = rec_s[...].astype(F32)
     attend((x,), [own_q[...]], own_kv[0:QK, :].T, own_kv[QK:, :], True)
@@ -434,7 +445,6 @@
         go_send(x_msg(d, x))
     go_send(q_msg(2, x))
     poll(1, first_half)
-    poll(1, second_half)
 
     cx[x] = mine_x[...]
     for d in range(1, NX):
@@ -456,6 +466,7 @@
     for d in (4, 3, 5, 2, 6, 1, 7):
         go_send(z_msg(d, z))
 
+    poll(1, second_half)
     poll(2, first_half)
     qs[x] = own_q[...]
     for d in (1, 3, 2):
@@ -465,11 +476,6 @@
         @pl.when(x < xx)
         def _():
             attend((xx,), [qs[xx]], own_kv[0:QK, :].T, own_kv[QK:, :], False)
-
-    poll(2, second_half)
-    below(1)
-    poll(3, first_half)
-    above(1)
 
     cz[z] = mine_z[...]
     for d in range(1, NZ):
@@ -480,22 +486,22 @@
     entering = pa * entering + pb
     state = loc_s[...] + cum_s[...] * entering
     rec = state * jax.nn.gelu(gate_s[...])
-    act_r[...] = (rec * rgain[...]).astype(BF16)
+    branch_r.begin((rec * rgain[...]).astype(BF16))
     square = (rec * rec).T
     sums[0:1, :] = jnp.sum(square, axis=0, keepdims=True)
-    for k in (0, 1):
-        branch_r.product(k)
+    poll(2, second_half)
+    below(1)
+    branch_r.send_far()
+    poll(3, first_half)
+    branch_r.send_pure()
+    above(1)
     poll(3, second_half)
-    for k in (2, 3):
-        branch_r.product(k)
-    branch_r.send_far()
     below(2)
-    poll(4, first_half)
-    branch_r.send_pure()
     above(2)
     below(3)
+    above(3)
+    poll(4, first_half)
     poll(4, second_half)
-    above(3)
     below(4)
 
     def o_msg(d):
@@ -536,12 +542,8 @@
     pl.semaphore_wait(hi.at[3], 1)
     for d in (4, 3, 5, 2, 6, 1, 7):
         go_send(sum_msg(d))
-    act_t[...] = (out.T * again[...]).astype(BF16)
-    branch_t.product(0)
-    branch_t.product(1)
+    branch_t.begin((out.T * again[...]).astype(BF16))
     branch_t.send_far()
-    branch_t.product(2)
-    branch_t.product(3)
     branch_t.send_pure()
     total = sums[...]
     for d in range(1, NT):
@@ -569,10 +571,10 @@
     scratch = [
         vm((NT, rows, depth), BF16), vm((1, model), F32), vm((model, 256), BF16),
         vm((QK + ROPE, model), BF16), vm((model, 512), BF16), vm((512, NOPE + VDIM), BF16),
-        vm((1, 512), F32), vm((ROPE // 2, rows), F32), vm((ROPE // 2, rows), F32),
+        vm((1, 512), F32), vm((ROPE // 2, rows), F32), vm((ROPE // 2, rows), F32), vm((ROPE // 2, rows), F32),
         vm((1, rows), F32), vm((4, 128), F32), vm((128, 128), BF16), vm((128, 128), BF16),
-        vm((1, 128), F32), vm((1, 128), F32), vm((1, 128), F32), vm((128, model), BF16),
-        vm((128, model), BF16), vm((1, model), F32),
+        vm((1, 128), F32), vm((1, 128), F32), vm((1, 128), F32), vm((256, model), BF16),
+        vm((256, model), BF16), vm((1, model), F32),
         vm((rows, 256), F32), vm((rows, 256), F32), vm((rows, 512), F32), vm((rows, 128), F32),
         vm((QK + VDIM, rows), BF16), vm((QK, rows), BF16), vm((rows, 128), BF16),
         vm((rows, 128), F32), vm((NZ, QK + VDIM, rows), BF16), vm((NX, QK, rows), BF16),
@@ -582,27 +584,28 @@
         vm((2, 128), F32), vm((NX, 2, 128), F32), vm((2, 128), F32), vm((NZ, 2, 128), F32),
         vm((NX - 1, VDIM, rows), BF16), vm((NX - 1, 2, rows), F32),
         vm((NX - 1, VDIM, rows), BF16), vm((NX - 1, 2, rows), F32),
-        vm((rows, 128), BF16), vm((rows, 128), BF16), vm((2, rows), F32),
+        vm((2, rows), F32),
         vm((NT - 1, 2, rows), F32), vm((2, rows, 128), F32),
         vm((1, mine, model), F32),
         dma((len(LOADS),)), pltpu.SemaphoreType.REGULAR((9,)),
         dma((13,)), dma((13,)), dma((8 * PIECES,)), dma((8 * PIECES,)),
         dma((NX - 1,)), dma((NX - 1,)), dma((2,)), dma((NX - 1,)), dma((NX - 1,)),
         dma((8,)), dma((8,)), dma((NX - 1,)), dma((NX - 1,)), dma((NX - 1,)), dma((NX - 1,)),
-        dma((NT - 1,)), dma((NT - 1,)),
+        dma((NT - 1,)), dma((NT - 1,)), dma((2,)), dma((2,)),
     ]
     for _ in range(2):
         scratch += [
-            vm((NY, mine, model), BF16), vm((NY, mine, model), BF16), vm((NY, mine, model), F32),
+            vm((rows, 128), BF16), vm((NY * mine, 128), BF16), vm((NY * mine, 256), BF16),
+            vm((3 * mine, model), F32),
             vm((mine, model), BF16), vm((mine, model), BF16),
             vm((2, mine, model), BF16), vm((2, mine, model), BF16),
         ]
     for _ in range(2):
-        scratch += [dma((NY,)), dma((NY,)), dma((2,)), dma((2,)), dma((4,)), dma((4,))]
+        scratch += [dma((1,)), dma((1,)), dma((2,)), dma((2,)), dma((4,)), dma((4,))]
     return pl.pallas_call(
         layer,
         name="layer",
-        out_shape=jax.ShapeDtypeStruct((mine, model), BF16),
+        out_shape=pltpu.VMEM((mine, model), BF16),
         in_specs=[pl.BlockSpec(memory_space=pl.ANY)] * len(LOADS),
         out_specs=pl.BlockSpec(memory_space=pltpu.VMEM),
         scratch_shapes=scratch,
@@ -618,13 +621,13 @@
     w_out_rec, w_out_att, post_gain,
 ):
     rows = tokens.shape[0]
-    frequency = 1.0 / THETA ** (jnp.arange(0, ROPE, 2).astype(F32) / ROPE)
-    places = (lax.axis_index("sp") * rows + jnp.arange(rows)).astype(F32)
-    turned = places[None, :] * frequency[:, None]
+    power = np.arange(0, ROPE, 2).astype(np.float32) / np.float32(ROPE)
+    frequency = np.float32(1.0) / np.float32(THETA) ** power
+    frequency = np.repeat(frequency[:, None], rows, axis=1)
     given = {
         "tok": tokens, "gain": pre_gain[None], "w_in": w_rec_in, "w_gate": w_rec_gate,
         "w_q": w_query.T, "w_rope": w_rope_key.T, "w_lat": w_latent, "w_exp": w_expand,
-        "lat_gain": latent_gain[None], "cos": jnp.cos(turned), "sin": jnp.sin(turned),
+        "lat_gain": latent_gain[None], "freq": jnp.asarray(frequency),
         "rf": rate_factor[None], "taps": conv_taps, "rmap": rate_maps[0], "imap": input_maps[0],
         "decay": decay_param[None], "rgain": rec_gain[None], "again": att_gain[None],
         "w_rec": w_out_rec, "w_att": w_out_att, "post": post_gain[None],

time: 62.1 us -> 59.9 us (0.965)
  local copies, waits for them, and re-layouts: 1.67 us -> 0.71 us
  other arithmetic: 0.84 us -> 0 us
    unnamed x1, local copies, waits for them, and re-layouts: 1.67 us -> 0.71 us
    sin x1 -> x0, other arithmetic: 0.82 us -> none  [shards(): jnp.sin(turned)]
where the time goes in v4:
time: 59.9 us; the launch traced here: 59.7 us
  Pallas kernels  59 us (98%)
  local copies, waits for them, and re-layouts  0.71 us (1%)
    pallas_call x1, Pallas kernels, call_layer(): pl.pallas_call(layer, name='layer', out_shape=pltpu.VMEM((mine, model), B...  59 us

profile of v4, /device:TPU:1, one launch (start us, length us, event | category | flops | bytes accessed | tf_op | source)
XLA Modules:
  0.0 59.7 jit_solution(10033857650674008382)
XLA Ops:
  0.0 59.0 %layer.1 = bf16[32,4096]{1,0:T(8,128)(2,1)S(1)} custom-call(bf16[256,512]{1,0:T(8,128)(2,1)} %refs_0_.1, f32[1,4096]{1,0:T(1,128)} %bitcast.15, bf16[4096,128]{1,0:T(8,128)(2,1)} %refs_2_.1, bf16[4096,128]{1,0:T(8,128)(2,1)} %refs_3_.1, bf16[192,4096]{1,0:T(8,128)(2,1)} %bitcast.11, bf16[64,4096]{1,0:T(8,128)(2,1)} %bitcast.12, bf16[4096,512]{1,0:T(8,128)(2,1)} %refs_6_.1, ...), custom_call_target="tpu_custom_call" | custom-call | tf_op jit(solution)/shard_map/layer/pallas_call | solution.py:605
  59.0 0.7 %copy.22 = bf16[32,4096]{1,0:T(8,128)(2,1)} copy(bf16[32,4096]{1,0:T(8,128)(2,1)S(1)} %layer.1) | data formatting | bytes 524288

commit v5 on v4

--- a/solution.py
+++ b/solution.py
@@ -81,14 +81,14 @@
     src = dict(zip(LOADS, refs[:n_in]))
     out_ref = refs[n_in]
     (
-        tok, gain, v_ig, v_qr, v_lat, v_exp, lat_gain, freq, cos_s, sin_s, rf, taps, rmap, imap, decay,
+        tok, gain, v_ig, v_qr, v_lat, v_exp, lat_gain, freq, cos_s, sin_s, cos_q, sin_q, rf, taps, rmap, imap, decay,
         rgain, again, w_rec, w_att, post,
         a_ig, a_qr, a_lat, sq,
         own_kv, own_q, rec_s, gate_s, kv, qs, halo, ext, m_s, l_s, o_s, cum_s, loc_s,
         mine_x, cx, mine_z, cz, po, ps, go, gs,
-        sums, got_s, inv_s, part,
+        sums, got_s, inv_s, sums_t, got_t, inv_t, both, part,
         lsem, hi, ass, ars, kss, krs, qss, qrs, hsem, xss, xrs, zss, zrs, oss, ors, tss, trs,
-        sss, srs, wss, wrs, *rest,
+        sss, srs, wss, wrs, uss, urs, *rest,
     ) = refs[n_in + 1 :]
     r_bufs, t_bufs = rest[0:8], rest[8:16]
     r_sems, t_sems = rest[16:22], rest[22:28]
@@ -120,7 +120,7 @@
         "w_gate": v_ig.at[:, pl.ds(128, 128)], "w_q": v_qr.at[pl.ds(0, QK)],
         "w_rope": v_qr.at[pl.ds(QK, ROPE)], "w_lat": v_lat, "w_exp": v_exp, "lat_gain": lat_gain,
         "freq": freq, "rf": rf, "taps": taps, "rmap": rmap, "imap": imap,
-        "decay": decay, "rgain": rgain, "again": again, "w_rec": w_rec.at[mine_rows], "w_att": w_att.at[mine_rows], "post": post,
+        "decay": decay, "rgain": rgain, "again": again.at[c], "w_rec": w_rec.at[mine_rows], "w_att": w_att.at[mine_rows], "post": post,
     }
     load = {
         name: pltpu.make_async_copy(src[name], where[name], lsem.at[k])
@@ -151,6 +151,17 @@
 
     def arrived(k, slot, piece):
         tok_msg(k, slot, piece, sib).wait_recv()
+
+    mine = out_ref.shape[0]
+
+    def query_place(shape):
+        lane = lax.broadcasted_iota(jnp.int32, shape, 1)
+        inner = lane % (NY * mine)
+        return (inner // mine) * (2 * mine) + (lane // (NY * mine)) * mine + inner % mine
+
+    def query_order(value):
+        starts = [(2 * yy + cc) * mine for cc in (0, 1) for yy in range(NY)]
+        return jnp.concatenate([value[k : k + mine] for k in starts], axis=0)
 
     load["tok"].wait()
     send(1, tp, h0, up)
@@ -183,6 +194,7 @@
     chunk(tp, True)
     pl.semaphore_wait(hi.at[2], 1)
     hello(hi.at[3], {"tp": dn})
+    hello(hi.at[9], xs[3])
     pl.semaphore_wait(hi.at[4], 1)
     hello(hi.at[6], zdn)
     pl.semaphore_wait(hi.at[5], 1)
@@ -195,6 +207,9 @@
     angle = places.astype(F32) * freq[...]
     cos_s[...] = jnp.cos(angle)
     sin_s[...] = jnp.sin(angle)
+    angle = (query_place((ROPE // 2, rows)) + sp * rows).astype(F32) * freq[...]
+    cos_q[...] = jnp.cos(angle)
+    sin_q[...] = jnp.sin(angle)
     arrived(1, dn, h0)
     send(5, dn, h0, up)
     send(7, dn, h0, sib)
@@ -275,8 +290,16 @@
     go_send(w_msg(w_rec, 0))
     go_send(w_msg(w_att, 1))
 
+    def gain_msg():
+        return remote(again.at[c], again.at[c], wss.at[2], wrs.at[2], {"tp": sib})
+
+    go_send(gain_msg())
+
+    query = query_order(inverse * a_qr[...])
+    turned = query[:, NOPE:].T
+    cosine, sine = cos_q[...], sin_q[...]
     u, w = turned[0:hr], turned[hr:ROPE]
-    own_q[0:NOPE, :] = (inverse * a_qr[:, 0:NOPE]).T.astype(BF16)
+    own_q[0:NOPE, :] = query[:, 0:NOPE].T.astype(BF16)
     own_q[NOPE : NOPE + hr, :] = (u * cosine - w * sine).astype(BF16)
     own_q[NOPE + hr :, :] = (w * cosine + u * sine).astype(BF16)
 
@@ -300,7 +323,7 @@
         scores = [mm(keys, query) * scale for query in queries]
         if masked:
             key = lax.broadcasted_iota(jnp.int32, scores[0].shape, 0)
-            place = lax.broadcasted_iota(jnp.int32, scores[0].shape, 1)
+            place = query_place(scores[0].shape)
             scores = [jnp.where(key <= place, s, LOW) for s in scores]
         before = [m_s[k] for k in slots]
         most = [jnp.maximum(b, jnp.max(s, axis=0, keepdims=True)) for b, s in zip(before, scores)]
@@ -343,7 +366,6 @@
         against((z + hop) % NZ)
 
     order = [(y + 2) % NY, (y + 1) % NY, (y + 3) % NY, y]
-    mine = out_ref.shape[0]
     middle = model // 2
     left, right = pl.ds(0, middle), pl.ds(middle, middle)
 
@@ -384,7 +406,6 @@
 
         def send_far(self):
             w_msg(self.weight, self.k).wait_recv()
-            self.pair().wait_recv()
             self.f_out[...] = mm(self.act[0:mine, :], self.weight[...]).astype(BF16)
             go_send(self.far(0))
             go_send(self.far(1))
@@ -445,6 +466,7 @@
         go_send(x_msg(d, x))
     go_send(q_msg(2, x))
     poll(1, first_half)
+    poll(1, second_half)
 
     cx[x] = mine_x[...]
     for d in range(1, NX):
@@ -466,7 +488,6 @@
     for d in (4, 3, 5, 2, 6, 1, 7):
         go_send(z_msg(d, z))
 
-    poll(1, second_half)
     poll(2, first_half)
     qs[x] = own_q[...]
     for d in (1, 3, 2):
@@ -476,6 +497,10 @@
         @pl.when(x < xx)
         def _():
             attend((xx,), [qs[xx]], own_kv[0:QK, :].T, own_kv[QK:, :], False)
+
+    poll(2, second_half)
+    below(1)
+    poll(3, first_half)
 
     cz[z] = mine_z[...]
     for d in range(1, NZ):
@@ -488,74 +513,108 @@
     rec = state * jax.nn.gelu(gate_s[...])
     branch_r.begin((rec * rgain[...]).astype(BF16))
     square = (rec * rec).T
-    sums[0:1, :] = jnp.sum(square, axis=0, keepdims=True)
-    poll(2, second_half)
-    below(1)
+    sums[...] = jnp.sum(square, axis=0, keepdims=True)
+
+    def sum_msg(d):
+        return remote(sums, got_s.at[d - 1], sss.at[d - 1], srs.at[d - 1], {"tp": (tp + d) % NT})
+
+    pl.semaphore_wait(hi.at[3], 1)
+    for d in (4, 3, 5, 2, 6, 1, 7):
+        go_send(sum_msg(d))
+    above(1)
+    branch_r.pair().wait_recv()
     branch_r.send_far()
-    poll(3, first_half)
     branch_r.send_pure()
-    above(1)
-    poll(3, second_half)
     below(2)
     above(2)
+    poll(3, second_half)
     below(3)
     above(3)
     poll(4, first_half)
     poll(4, second_half)
     below(4)
 
-    def o_msg(d):
-        return remote(po.at[d - 1], go.at[d - 1], oss.at[d - 1], ors.at[d - 1], xs[d])
-
-    def s_msg(d):
-        return remote(ps.at[d - 1], gs.at[d - 1], tss.at[d - 1], trs.at[d - 1], xs[d])
-
-    for d in (2, 1, 3):
-        xx = (x + d) % NX
-        total = l_s[xx]
-        ps[d - 1, 0:1, :] = m_s[xx]
-        ps[d - 1, 1:2, :] = total
-        po[d - 1] = (o_s[xx] / jnp.where(total > 0.0, total, 1.0)).astype(BF16)
-        go_send(s_msg(d))
-        go_send(o_msg(d))
-
+    lanes = NY * mine
+
+    def part_to(d, e):
+        return {"sp": z * NX + (x + d) % NX, "tp": sib if e else tp}
+
+    def o_msg(d, e):
+        k = d * 2 + e
+        return remote(po.at[k], go.at[k], oss.at[k], ors.at[k], part_to(d, e))
+
+    def s_msg(d, e):
+        k = d * 2 + e
+        return remote(ps.at[k], gs.at[k], tss.at[k], trs.at[k], part_to(d, e))
+
+    pl.semaphore_wait(hi.at[9], 1)
+    for d, e in ((2, 0), (2, 1), (1, 0), (3, 0), (1, 1), (3, 1), (0, 1)):
+        k, xx = d * 2 + e, (x + d) % NX
+        at = pl.ds(pl.multiple_of((c + e - 2 * c * e) * lanes, lanes), lanes)
+        total = l_s[xx, :, at]
+        ps[k, 0:1, :] = m_s[xx, :, at]
+        ps[k, 1:2, :] = total
+        po[k] = (o_s[xx, :, at] / jnp.where(total > 0.0, total, 1.0)).astype(BF16)
+        go_send(s_msg(d, e))
+        go_send(o_msg(d, e))
     branch_r.send_joined()
 
-    most = m_s[x]
-    for d in range(1, NX):
-        s_msg(d).wait_recv()
-        most = jnp.maximum(most, gs[d - 1, 0:1, :])
-    share = jnp.exp2(m_s[x] - most)
-    total = l_s[x] * share
-    out = o_s[x] * share
-    for d in range(1, NX):
-        o_msg(d).wait_recv()
-        share = gs[d - 1, 1:2, :] * jnp.exp2(gs[d - 1, 0:1, :] - most)
-        total = total + share
-        out = out + go[d - 1].astype(F32) * share
-    out = out / total
-    sums[1:2, :] = jnp.sum(out * out, axis=0, keepdims=True)
-
-    def sum_msg(d):
-        return remote(sums, got_s.at[d - 1], sss.at[d - 1], srs.at[d - 1], {"tp": (tp + d) % NT})
-
-    pl.semaphore_wait(hi.at[3], 1)
-    for d in (4, 3, 5, 2, 6, 1, 7):
-        go_send(sum_msg(d))
-    branch_t.begin((out.T * again[...]).astype(BF16))
+    mine_lanes = pl.ds(pl.multiple_of(c * lanes, lanes), lanes)
+    gain_msg().wait_recv()
+    squares = jnp.zeros((1, lanes), F32)
+    for e in (0, 1):
+        if e == 0:
+            most = m_s[x, :, mine_lanes]
+        else:
+            s_msg(0, 1).wait_recv()
+            most = gs[1, 0:1, :]
+        for d in range(1, NX):
+            s_msg(d, e).wait_recv()
+            most = jnp.maximum(most, gs[d * 2 + e, 0:1, :])
+        total, out = jnp.zeros((1, lanes), F32), jnp.zeros((VDIM, lanes), F32)
+        for d in range(NX):
+            k = d * 2 + e
+            if k == 0:
+                share = jnp.exp2(m_s[x, :, mine_lanes] - most)
+                total = l_s[x, :, mine_lanes] * share
+                out = o_s[x, :, mine_lanes] * share
+            else:
+                o_msg(d, e).wait_recv()
+                share = gs[k, 1:2, :] * jnp.exp2(gs[k, 0:1, :] - most)
+                total = total + share
+                out = out + go[k].astype(F32) * share
+        out = out / total
+        squares = squares + jnp.sum(out * out, axis=0, keepdims=True)
+        head = c + e - 2 * c * e
+        at = pl.ds(pl.multiple_of(head * 128, 128), 128)
+        both[:, at] = (out.T * again[head]).astype(BF16)
+    sums_t[...] = squares
+
+    def t_msg(k):
+        to = (up, dn, far)[k]
+        return remote(sums_t, got_t.at[k], uss.at[k], urs.at[k], {"tp": to})
+
+    for k in (2, 0, 1):
+        go_send(t_msg(k))
+    for k, yy in enumerate(order):
+        at = pl.ds(pl.multiple_of(yy * mine, mine), mine)
+        branch_t.act[k * mine : (k + 1) * mine, :] = both[at, :]
     branch_t.send_far()
     branch_t.send_pure()
     total = sums[...]
     for d in range(1, NT):
         sum_msg(d).wait_recv()
         total = total + got_s[d - 1]
-    inverse = lax.rsqrt(total / (128 * NT) + EPS)
-    inv_s[0] = jnp.broadcast_to(inverse[0:1, :], (128, rows)).T
-    inv_s[1] = jnp.broadcast_to(inverse[1:2, :], (128, rows)).T
-    at = rows_of(y, c)
-    part[0] = branch_r.total() * inv_s[0, at, :][:, 0:1]
+    inv_s[...] = jnp.broadcast_to(lax.rsqrt(total / (128 * NT) + EPS), (128, rows)).T
+    part[0] = branch_r.total() * inv_s[rows_of(y, c), :][:, 0:1]
+    total = sums_t[...]
+    for k in range(NY - 1):
+        t_msg(k).wait_recv()
+        total = total + got_t[k]
+    inv_t[...] = jnp.broadcast_to(lax.rsqrt(total / (128 * NT) + EPS), (128, lanes)).T
     branch_t.send_joined()
-    mixed = part[0] + branch_t.total() * inv_s[1, at, :][:, 0:1]
+    at = pl.ds(pl.multiple_of(y * mine, mine), mine)
+    mixed = part[0] + branch_t.total() * inv_t[at, :][:, 0:1]
     spread = lax.rsqrt(jnp.mean(mixed * mixed, axis=1, keepdims=True) + EPS)
     out_ref[...] = (mixed * spread * post[...]).astype(BF16)
     for copy in sent:
@@ -571,9 +630,9 @@
     scratch = [
         vm((NT, rows, depth), BF16), vm((1, model), F32), vm((model, 256), BF16),
         vm((QK + ROPE, model), BF16), vm((model, 512), BF16), vm((512, NOPE + VDIM), BF16),
-        vm((1, 512), F32), vm((ROPE // 2, rows), F32), vm((ROPE // 2, rows), F32), vm((ROPE // 2, rows), F32),
+        vm((1, 512), F32), *[vm((ROPE // 2, rows), F32) for _ in range(5)],
         vm((1, rows), F32), vm((4, 128), F32), vm((128, 128), BF16), vm((128, 128), BF16),
-        vm((1, 128), F32), vm((1, 128), F32), vm((1, 128), F32), vm((256, model), BF16),
+        vm((1, 128), F32), vm((1, 128), F32), vm((2, 1, 128), F32), vm((256, model), BF16),
         vm((256, model), BF16), vm((1, model), F32),
         vm((rows, 256), F32), vm((rows, 256), F32), vm((rows, 512), F32), vm((rows, 128), F32),
         vm((QK + VDIM, rows), BF16), vm((QK, rows), BF16), vm((rows, 128), BF16),
@@ -582,16 +641,17 @@
         vm((NX, 1, rows), F32), vm((NX, VDIM, rows), F32), vm((rows, 128), F32),
         vm((rows, 128), F32),
         vm((2, 128), F32), vm((NX, 2, 128), F32), vm((2, 128), F32), vm((NZ, 2, 128), F32),
-        vm((NX - 1, VDIM, rows), BF16), vm((NX - 1, 2, rows), F32),
-        vm((NX - 1, VDIM, rows), BF16), vm((NX - 1, 2, rows), F32),
-        vm((2, rows), F32),
-        vm((NT - 1, 2, rows), F32), vm((2, rows, 128), F32),
+        vm((2 * NX, VDIM, NY * mine), BF16), vm((2 * NX, 2, NY * mine), F32),
+        vm((2 * NX, VDIM, NY * mine), BF16), vm((2 * NX, 2, NY * mine), F32),
+        vm((1, rows), F32), vm((NT - 1, 1, rows), F32), vm((rows, 128), F32),
+        vm((1, NY * mine), F32), vm((NY - 1, 1, NY * mine), F32), vm((NY * mine, 128), F32),
+        vm((NY * mine, 256), BF16),
         vm((1, mine, model), F32),
-        dma((len(LOADS),)), pltpu.SemaphoreType.REGULAR((9,)),
+        dma((len(LOADS),)), pltpu.SemaphoreType.REGULAR((10,)),
         dma((13,)), dma((13,)), dma((8 * PIECES,)), dma((8 * PIECES,)),
         dma((NX - 1,)), dma((NX - 1,)), dma((2,)), dma((NX - 1,)), dma((NX - 1,)),
-        dma((8,)), dma((8,)), dma((NX - 1,)), dma((NX - 1,)), dma((NX - 1,)), dma((NX - 1,)),
-        dma((NT - 1,)), dma((NT - 1,)), dma((2,)), dma((2,)),
+        dma((8,)), dma((8,)), dma((2 * NX,)), dma((2 * NX,)), dma((2 * NX,)), dma((2 * NX,)),
+        dma((NT - 1,)), dma((NT - 1,)), dma((3,)), dma((3,)), dma((NY - 1,)), dma((NY - 1,)),
     ]
     for _ in range(2):
         scratch += [

time: 59.9 us -> 57.8 us (0.965)
  Pallas kernels: 59 us -> 56.9 us
    pallas_call x1, Pallas kernels: 59 us -> 56.9 us  [call_layer(): pl.pallas_call(layer, name='layer', out_shape=pltpu.VMEM((mine, model), B...]
where the time goes in v5:
time: 57.8 us; the launch traced here: 57.7 us
  Pallas kernels  56.9 us (98%)
  local copies, waits for them, and re-layouts  0.71 us (1%)
    pallas_call x1, Pallas kernels, call_layer(): pl.pallas_call(layer, name='layer', out_shape=pltpu.VMEM((mine, model), B...  56.9 us

profile of v5, /device:TPU:1, one launch (start us, length us, event | category | flops | bytes accessed | tf_op | source)
XLA Modules:
  0.0 57.7 jit_solution(1878474266772631189)
XLA Ops:
  0.0 56.9 %layer.1 = bf16[32,4096]{1,0:T(8,128)(2,1)S(1)} custom-call(bf16[256,512]{1,0:T(8,128)(2,1)} %refs_0_.1, f32[1,4096]{1,0:T(1,128)} %bitcast.15, bf16[4096,128]{1,0:T(8,128)(2,1)} %refs_2_.1, bf16[4096,128]{1,0:T(8,128)(2,1)} %refs_3_.1, bf16[192,4096]{1,0:T(8,128)(2,1)} %bitcast.11, bf16[64,4096]{1,0:T(8,128)(2,1)} %bitcast.12, bf16[4096,512]{1,0:T(8,128)(2,1)} %refs_6_.1, ...), custom_call_target="tpu_custom_call" | custom-call | tf_op jit(solution)/shard_map/layer/pallas_call | solution.py:665
  57.0 0.7 %copy.22 = bf16[32,4096]{1,0:T(8,128)(2,1)} copy(bf16[32,4096]{1,0:T(8,128)(2,1)S(1)} %layer.1) | data formatting | bytes 524288

commit v6 on v5

--- a/solution.py
+++ b/solution.py
@@ -85,7 +85,7 @@
         rgain, again, w_rec, w_att, post,
         a_ig, a_qr, a_lat, sq,
         own_kv, own_q, rec_s, gate_s, kv, qs, halo, ext, m_s, l_s, o_s, cum_s, loc_s,
-        mine_x, cx, mine_z, cz, po, ps, go, gs,
+        mine_x, cx, mine_z, cz, pre_x, ent_s, po, ps, go, gs,
         sums, got_s, inv_s, sums_t, got_t, inv_t, both, part,
         lsem, hi, ass, ars, kss, krs, qss, qrs, hsem, xss, xrs, zss, zrs, oss, ors, tss, trs,
         sss, srs, wss, wrs, uss, urs, *rest,
@@ -373,8 +373,8 @@
         return pl.ds(pl.multiple_of((yy * 2 + cc) * mine, mine), mine)
 
     class Branch:
-        def __init__(self, weight, k, bufs, sems):
-            self.weight, self.k = weight, k
+        def __init__(self, weight, k, bufs, sems, go):
+            self.weight, self.k, self.go = weight, k, go
             self.natural, self.out, self.act, self.own, self.f_out, self.f_in, self.n_out, self.n_in = bufs
             self.ps, self.pr, self.fs, self.fr, self.ns, self.nr = sems
 
@@ -402,20 +402,20 @@
                 at = slice(k * mine, (k + 1) * mine)
                 self.out[at, :] = self.natural[rows_of(yy, 1 - c), :]
                 self.act[at, mine_rows] = self.natural[rows_of(yy, c), :]
-            go_send(self.pair())
+            self.go(self.pair())
 
         def send_far(self):
             w_msg(self.weight, self.k).wait_recv()
             self.f_out[...] = mm(self.act[0:mine, :], self.weight[...]).astype(BF16)
-            go_send(self.far(0))
-            go_send(self.far(1))
+            self.go(self.far(0))
+            self.go(self.far(1))
 
         def send_pure(self):
             self.own[...] = mm(self.act[mine:, :], self.weight[...])
             self.n_out[0, :, middle:] = self.own[0:mine, middle:].astype(BF16)
-            go_send(self.near(0))
+            self.go(self.near(0))
             self.n_out[1, :, 0:middle] = self.own[mine : 2 * mine, 0:middle].astype(BF16)
-            go_send(self.near(1))
+            self.go(self.near(1))
 
         def send_joined(self):
             self.far(0).wait_recv()
@@ -432,8 +432,8 @@
                 self.near(k).wait_recv()
             return self.own[2 * mine :, :] + self.n_in[0].astype(F32) + self.n_in[1].astype(F32)
 
-    branch_r = Branch(w_rec, 0, r_bufs, r_sems)
-    branch_t = Branch(w_att, 1, t_bufs, t_sems)
+    branch_r = Branch(w_rec, 0, r_bufs, r_sems, lambda copy: copy.start())
+    branch_t = Branch(w_att, 1, t_bufs, t_sems, go_send)
 
     ext[16:, :] = rec_s[...].astype(F32)
     attend((x,), [own_q[...]], own_kv[0:QK, :].T, own_kv[QK:, :], True)
@@ -478,6 +478,8 @@
         ta, tb = ta * a, a * tb + b
         pa = jnp.where(i < x, pa * a, pa)
         pb = jnp.where(i < x, a * pb + b, pb)
+    pre_x[0:1, :] = pa
+    pre_x[1:2, :] = pb
     mine_z[0:1, :] = ta
     mine_z[1:2, :] = tb
 
@@ -498,22 +500,43 @@
         def _():
             attend((xx,), [qs[xx]], own_kv[0:QK, :].T, own_kv[QK:, :], False)
 
+    def carried(d):
+        z_msg(d, (z + NZ - d) % NZ).wait_recv()
+
+    def whole_recurrence():
+        for d in range(1, NZ):
+
+            @pl.when(d <= z)
+            def _():
+                carried(d)
+
+        ent_s[...] = jnp.zeros((1, 128), F32)
+        for i in range(NZ - 1):
+
+            @pl.when(i < z)
+            def _():
+                ent_s[...] = cz[i, 0:1, :] * ent_s[...] + cz[i, 1:2, :]
+
+        entering = pre_x[0:1, :] * ent_s[...] + pre_x[1:2, :]
+        state = loc_s[...] + cum_s[...] * entering
+        rec = state * jax.nn.gelu(gate_s[...])
+        branch_r.begin((rec * rgain[...]).astype(BF16))
+        square = (rec * rec).T
+        sums[...] = jnp.sum(square, axis=0, keepdims=True)
+
+    def reduce_r():
+        branch_r.pair().wait_recv()
+        branch_r.send_far()
+        branch_r.send_pure()
+
+    early = z < NZ // 2
+    late = z >= NZ // 2
     poll(2, second_half)
+    pl.when(early)(whole_recurrence)
     below(1)
+    pl.when(early)(reduce_r)
     poll(3, first_half)
-
-    cz[z] = mine_z[...]
-    for d in range(1, NZ):
-        z_msg(d, (z + NZ - d) % NZ).wait_recv()
-    entering = jnp.zeros((1, 128), F32)
-    for i in range(NZ):
-        entering = jnp.where(i < z, cz[i, 0:1, :] * entering + cz[i, 1:2, :], entering)
-    entering = pa * entering + pb
-    state = loc_s[...] + cum_s[...] * entering
-    rec = state * jax.nn.gelu(gate_s[...])
-    branch_r.begin((rec * rgain[...]).astype(BF16))
-    square = (rec * rec).T
-    sums[...] = jnp.sum(square, axis=0, keepdims=True)
+    pl.when(late)(whole_recurrence)
 
     def sum_msg(d):
         return remote(sums, got_s.at[d - 1], sss.at[d - 1], srs.at[d - 1], {"tp": (tp + d) % NT})
@@ -522,41 +545,52 @@
     for d in (4, 3, 5, 2, 6, 1, 7):
         go_send(sum_msg(d))
     above(1)
-    branch_r.pair().wait_recv()
-    branch_r.send_far()
-    branch_r.send_pure()
+    pl.when(late)(reduce_r)
+    sent.append(branch_r.pair())
+    for k in (0, 1):
+        sent.append(branch_r.far(k))
+        sent.append(branch_r.near(k))
     below(2)
     above(2)
     poll(3, second_half)
     below(3)
+
+    lanes = NY * mine
+
+    def part_to(d, e):
+        return {"sp": z * NX + (x + d) % NX, "tp": sib if e else tp}
+
+    def o_msg(d, e):
+        k = d * 2 + e
+        return remote(po.at[k], go.at[k], oss.at[k], ors.at[k], part_to(d, e))
+
+    def s_msg(d, e):
+        k = d * 2 + e
+        return remote(ps.at[k], gs.at[k], tss.at[k], trs.at[k], part_to(d, e))
+
+    pl.semaphore_wait(hi.at[9], 1)
+    others = ((2, 0), (2, 1), (1, 0), (3, 0), (1, 1), (3, 1), (0, 1))
+
+    def send_outputs():
+        for d, e in others:
+            k, xx = d * 2 + e, (x + d) % NX
+            at = pl.ds(pl.multiple_of((c + e - 2 * c * e) * lanes, lanes), lanes)
+            total = l_s[xx, :, at]
+            ps[k, 0:1, :] = m_s[xx, :, at]
+            ps[k, 1:2, :] = total
+            po[k] = (o_s[xx, :, at] / jnp.where(total > 0.0, total, 1.0)).astype(BF16)
+            s_msg(d, e).start()
+            o_msg(d, e).start()
+
+    pl.when(early)(send_outputs)
     above(3)
     poll(4, first_half)
     poll(4, second_half)
     below(4)
-
-    lanes = NY * mine
-
-    def part_to(d, e):
-        return {"sp": z * NX + (x + d) % NX, "tp": sib if e else tp}
-
-    def o_msg(d, e):
-        k = d * 2 + e
-        return remote(po.at[k], go.at[k], oss.at[k], ors.at[k], part_to(d, e))
-
-    def s_msg(d, e):
-        k = d * 2 + e
-        return remote(ps.at[k], gs.at[k], tss.at[k], trs.at[k], part_to(d, e))
-
-    pl.semaphore_wait(hi.at[9], 1)
-    for d, e in ((2, 0), (2, 1), (1, 0), (3, 0), (1, 1), (3, 1), (0, 1)):
-        k, xx = d * 2 + e, (x + d) % NX
-        at = pl.ds(pl.multiple_of((c + e - 2 * c * e) * lanes, lanes), lanes)
-        total = l_s[xx, :, at]
-        ps[k, 0:1, :] = m_s[xx, :, at]
-        ps[k, 1:2, :] = total
-        po[k] = (o_s[xx, :, at] / jnp.where(total > 0.0, total, 1.0)).astype(BF16)
-        go_send(s_msg(d, e))
-        go_send(o_msg(d, e))
+    pl.when(late)(send_outputs)
+    for d, e in others:
+        sent.append(s_msg(d, e))
+        sent.append(o_msg(d, e))
     branch_r.send_joined()
 
     mine_lanes = pl.ds(pl.multiple_of(c * lanes, lanes), lanes)
@@ -617,6 +651,12 @@
     mixed = part[0] + branch_t.total() * inv_t[at, :][:, 0:1]
     spread = lax.rsqrt(jnp.mean(mixed * mixed, axis=1, keepdims=True) + EPS)
     out_ref[...] = (mixed * spread * post[...]).astype(BF16)
+    for d in range(1, NZ):
+
+        @pl.when(d > z)
+        def _():
+            carried(d)
+
     for copy in sent:
         copy.wait_send()
 
@@ -641,6 +681,7 @@
         vm((NX, 1, rows), F32), vm((NX, VDIM, rows), F32), vm((rows, 128), F32),
         vm((rows, 128), F32),
         vm((2, 128), F32), vm((NX, 2, 128), F32), vm((2, 128), F32), vm((NZ, 2, 128), F32),
+        vm((2, 128), F32), vm((1, 128), F32),
         vm((2 * NX, VDIM, NY * mine), BF16), vm((2 * NX, 2, NY * mine), F32),
         vm((2 * NX, VDIM, NY * mine), BF16), vm((2 * NX, 2, NY * mine), F32),
         vm((1, rows), F32), vm((NT - 1, 1, rows), F32), vm((rows, 128), F32),

time: 57.8 us -> 55.9 us (0.967)
  Pallas kernels: 56.9 us -> 55 us
    pallas_call x1, Pallas kernels: 56.9 us -> 55 us  [call_layer(): pl.pallas_call(layer, name='layer', out_shape=pltpu.VMEM((mine, model), B...]
where the time goes in v6:
time: 55.9 us; the launch traced here: 55.8 us
  Pallas kernels  55 us (98%)
  local copies, waits for them, and re-layouts  0.71 us (1%)
    pallas_call x1, Pallas kernels, call_layer(): pl.pallas_call(layer, name='layer', out_shape=pltpu.VMEM((mine, model), B...  55 us

profile of v6, /device:TPU:1, one launch (start us, length us, event | category | flops | bytes accessed | tf_op | source)
XLA Modules:
  0.0 55.8 jit_solution(16185196589565987492)
XLA Ops:
  0.0 55.0 %layer.1 = bf16[32,4096]{1,0:T(8,128)(2,1)S(1)} custom-call(bf16[256,512]{1,0:T(8,128)(2,1)} %refs_0_.1, f32[1,4096]{1,0:T(1,128)} %bitcast.15, bf16[4096,128]{1,0:T(8,128)(2,1)} %refs_2_.1, bf16[4096,128]{1,0:T(8,128)(2,1)} %refs_3_.1, bf16[192,4096]{1,0:T(8,128)(2,1)} %bitcast.11, bf16[64,4096]{1,0:T(8,128)(2,1)} %bitcast.12, bf16[4096,512]{1,0:T(8,128)(2,1)} %refs_6_.1, ...), custom_call_target="tpu_custom_call" | custom-call | tf_op jit(solution)/shard_map/layer/pallas_call | solution.py:706
  55.1 0.7 %copy.22 = bf16[32,4096]{1,0:T(8,128)(2,1)} copy(bf16[32,4096]{1,0:T(8,128)(2,1)S(1)} %layer.1) | data formatting | bytes 524288

commit v7 on v6

--- a/solution.py
+++ b/solution.py
@@ -490,71 +490,6 @@
     for d in (4, 3, 5, 2, 6, 1, 7):
         go_send(z_msg(d, z))
 
-    poll(2, first_half)
-    qs[x] = own_q[...]
-    for d in (1, 3, 2):
-        q_msg(d, (x + NX - d) % NX).wait_recv()
-    for xx in range(1, NX):
-
-        @pl.when(x < xx)
-        def _():
-            attend((xx,), [qs[xx]], own_kv[0:QK, :].T, own_kv[QK:, :], False)
-
-    def carried(d):
-        z_msg(d, (z + NZ - d) % NZ).wait_recv()
-
-    def whole_recurrence():
-        for d in range(1, NZ):
-
-            @pl.when(d <= z)
-            def _():
-                carried(d)
-
-        ent_s[...] = jnp.zeros((1, 128), F32)
-        for i in range(NZ - 1):
-
-            @pl.when(i < z)
-            def _():
-                ent_s[...] = cz[i, 0:1, :] * ent_s[...] + cz[i, 1:2, :]
-
-        entering = pre_x[0:1, :] * ent_s[...] + pre_x[1:2, :]
-        state = loc_s[...] + cum_s[...] * entering
-        rec = state * jax.nn.gelu(gate_s[...])
-        branch_r.begin((rec * rgain[...]).astype(BF16))
-        square = (rec * rec).T
-        sums[...] = jnp.sum(square, axis=0, keepdims=True)
-
-    def reduce_r():
-        branch_r.pair().wait_recv()
-        branch_r.send_far()
-        branch_r.send_pure()
-
-    early = z < NZ // 2
-    late = z >= NZ // 2
-    poll(2, second_half)
-    pl.when(early)(whole_recurrence)
-    below(1)
-    pl.when(early)(reduce_r)
-    poll(3, first_half)
-    pl.when(late)(whole_recurrence)
-
-    def sum_msg(d):
-        return remote(sums, got_s.at[d - 1], sss.at[d - 1], srs.at[d - 1], {"tp": (tp + d) % NT})
-
-    pl.semaphore_wait(hi.at[3], 1)
-    for d in (4, 3, 5, 2, 6, 1, 7):
-        go_send(sum_msg(d))
-    above(1)
-    pl.when(late)(reduce_r)
-    sent.append(branch_r.pair())
-    for k in (0, 1):
-        sent.append(branch_r.far(k))
-        sent.append(branch_r.near(k))
-    below(2)
-    above(2)
-    poll(3, second_half)
-    below(3)
-
     lanes = NY * mine
 
     def part_to(d, e):
@@ -582,7 +517,77 @@
             s_msg(d, e).start()
             o_msg(d, e).start()
 
-    pl.when(early)(send_outputs)
+    def carried(d):
+        z_msg(d, (z + NZ - d) % NZ).wait_recv()
+
+    def whole_recurrence():
+        for d in range(1, NZ):
+
+            @pl.when(d <= z)
+            def _():
+                carried(d)
+
+        ent_s[...] = jnp.zeros((1, 128), F32)
+        for i in range(NZ - 1):
+
+            @pl.when(i < z)
+            def _():
+                ent_s[...] = cz[i, 0:1, :] * ent_s[...] + cz[i, 1:2, :]
+
+        entering = pre_x[0:1, :] * ent_s[...] + pre_x[1:2, :]
+        state = loc_s[...] + cum_s[...] * entering
+        rec = state * jax.nn.gelu(gate_s[...])
+        branch_r.begin((rec * rgain[...]).astype(BF16))
+        square = (rec * rec).T
+        sums[...] = jnp.sum(square, axis=0, keepdims=True)
+
+    def reduce_r():
+        branch_r.pair().wait_recv()
+        branch_r.send_far()
+        branch_r.send_pure()
+
+    pl.when(z == 0)(whole_recurrence)
+    poll(2, first_half)
+    pl.when(z == 0)(reduce_r)
+    qs[x] = own_q[...]
+    for d in (1, 3, 2):
+        q_msg(d, (x + NX - d) % NX).wait_recv()
+    for xx in range(1, NX):
+
+        @pl.when(x < xx)
+        def _():
+            attend((xx,), [qs[xx]], own_kv[0:QK, :].T, own_kv[QK:, :], False)
+
+    early = z < NZ // 2
+    late = z >= NZ // 2
+    pl.when(z == 0)(send_outputs)
+    below(1)
+    pl.when(z == 1)(send_outputs)
+    pl.when(z == 1)(whole_recurrence)
+    poll(2, second_half)
+    pl.when(jnp.logical_and(z >= 2, early))(whole_recurrence)
+    above(1)
+    pl.when(jnp.logical_and(z >= 1, early))(reduce_r)
+    poll(3, first_half)
+    pl.when(late)(whole_recurrence)
+
+    def sum_msg(d):
+        return remote(sums, got_s.at[d - 1], sss.at[d - 1], srs.at[d - 1], {"tp": (tp + d) % NT})
+
+    pl.semaphore_wait(hi.at[3], 1)
+    for d in (4, 3, 5, 2, 6, 1, 7):
+        go_send(sum_msg(d))
+    below(2)
+    pl.when(z == 2)(send_outputs)
+    pl.when(late)(reduce_r)
+    sent.append(branch_r.pair())
+    for k in (0, 1):
+        sent.append(branch_r.far(k))
+        sent.append(branch_r.near(k))
+    above(2)
+    poll(3, second_half)
+    below(3)
+    pl.when(z == 3)(send_outputs)
     above(3)
     poll(4, first_half)
     poll(4, second_half)

time: 55.9 us -> 54.9 us (0.982)
  Pallas kernels: 55 us -> 53.9 us
    pallas_call x1, Pallas kernels: 55 us -> 53.9 us  [call_layer(): pl.pallas_call(layer, name='layer', out_shape=pltpu.VMEM((mine, model), B...]
where the time goes in v7:
time: 54.9 us; the launch traced here: 54.6 us
  Pallas kernels  53.9 us (98%)
  local copies, waits for them, and re-layouts  0.71 us (1%)
    pallas_call x1, Pallas kernels, call_layer(): pl.pallas_call(layer, name='layer', out_shape=pltpu.VMEM((mine, model), B...  53.9 us

profile of v7, /device:TPU:1, one launch (start us, length us, event | category | flops | bytes accessed | tf_op | source)
XLA Modules:
  0.0 54.6 jit_solution(6179579427058715332)
XLA Ops:
  0.0 53.9 %layer.1 = bf16[32,4096]{1,0:T(8,128)(2,1)S(1)} custom-call(bf16[256,512]{1,0:T(8,128)(2,1)} %refs_0_.1, f32[1,4096]{1,0:T(1,128)} %bitcast.15, bf16[4096,128]{1,0:T(8,128)(2,1)} %refs_2_.1, bf16[4096,128]{1,0:T(8,128)(2,1)} %refs_3_.1, bf16[192,4096]{1,0:T(8,128)(2,1)} %bitcast.11, bf16[64,4096]{1,0:T(8,128)(2,1)} %bitcast.12, bf16[4096,512]{1,0:T(8,128)(2,1)} %refs_6_.1, ...), custom_call_target="tpu_custom_call" | custom-call | tf_op jit(solution)/shard_map/layer/pallas_call | solution.py:711
  53.9 0.7 %copy.22 = bf16[32,4096]{1,0:T(8,128)(2,1)} copy(bf16[32,4096]{1,0:T(8,128)(2,1)S(1)} %layer.1) | data formatting | bytes 524288
